TPU v7x, 32 devices: a whole 2x2x4 slice. The times are simulated.
32 devices in a mesh: rep: 2 (over x), fs: 8 (over z, y), tp: 2 (over core).
Axes of the slice: x: 2, y: 2, z: 4, core: 2. Of those that a mesh axis runs over, the one named last changes fastest.
Arguments:
- tokens: bfloat16 [16, 384, 2048], P(('rep', 'fs')), may hold values from -6 to 6
- mix_gain: float32 [2048], replicated, may hold values from 0.1 to 1.9
- value_weight: float32 [2048, 2048], P('fs', 'tp'), may hold values from -0.125 to 0.125
- value_scale: float32 [2048], P(('tp', 'fs')), may hold values from 0.5 to 2
- inner_weight: float32 [2048, 2048], P('fs', 'tp'), may hold values from -0.125 to 0.125
- inner_scale: float32 [2048], P(('tp', 'fs')), may hold values from 0.5 to 2
- outer_weight: float32 [2048, 2048], P('fs', 'tp'), may hold values from -0.125 to 0.125
- outer_scale: float32 [2048], P(('tp', 'fs')), may hold values from 0.5 to 2
- conv_taps: float32 [3, 2048], P(None, 'tp'), may hold values from -3 to 3
- out_weight: float32 [2048, 2048], P('tp', 'fs'), may hold values from -0.125 to 0.125
- out_scale: float32 [2048], P('fs'), may hold values from 0.5 to 2
- mlp_gain: float32 [2048], replicated, may hold values from 0.1 to 1.9
- up_weight: float32 [2048, 6144], P('fs', 'tp'), may hold values from -0.125 to 0.125
- up_scale: float32 [6144], P(('tp', 'fs')), may hold values from 0.5 to 2
- down_weight: float32 [6144, 2048], P('tp', 'fs'), may hold values from -0.078125 to 0.078125
- down_scale: float32 [2048], P('fs'), may hold values from 0.5 to 2
Outputs:
- layer_out: bfloat16 [16, 384, 2048], P(('rep', 'fs'))
All inputs are finite; a program needn't handle non-finite values.
Results may differ from a plain program's by a relative error of at most 0.02.
Values may be sent and summed in bfloat16 or wider, within the bound.
A program may use at most 128 MiB of HBM per device.

v0:
```python
import functools

import jax
import jax.numpy as jnp
from jax import lax
from jax.experimental import pallas as pl
from jax.experimental.pallas import tpu as pltpu
from jax.sharding import PartitionSpec as P

MESH = pl.DeviceIdType.MESH
norm_eps = 1e-06
HALO = 16
TILE = 16
f32 = jnp.float32
bf16 = jnp.bfloat16


def kernel(
    nz, G, T, win, rows, inside,
    tok, g1, g2, vectors, weights,
    out,
    WA, WO, WU, WD, nrm, hid, p1, q1, mid32, mid, act, p2, q2,
    staged, leaving, gathered,
    rz, rd, sz, sd, sy, loc, rn, sn, r1, s1, ra, sa, r2, s2, ro, so,
):
    if inside:
        packed, table, asc, taps, usc, oc, dc = gathered
    else:
        asc, taps, usc, oc, dc = vectors
    D = tok.shape[1]
    pw = D // nz
    cw = pw // 2
    r, f, t = lax.axis_index("rep"), lax.axis_index("fs"), lax.axis_index("tp")
    z, y = f // 2, f % 2
    fy = z * 2 + 1 - y
    g = r * 2 + y
    ka, ko, ku, kd = (w.shape[0] for w in leaving)
    stages = range(5 if inside else 4)
    has_lo, has_hi = z > 0, z < nz - 1
    if T == 2:
        start, off = t * (rows - HALO), t * HALO
    else:
        start = jnp.clip(t * rows - HALO, 0, tok.shape[0] - win)
        off = t * rows - start
    start, off = pl.multiple_of(start, HALO), pl.multiple_of(off, HALO)

    def member(m):
        return (m // 2, z * 2 + m % 2, t)

    def others():
        return [(g + d) % G for d in range(1, G)]

    def siblings():
        return [(t + d) % T for d in range(1, T)]

    def copy(src, dst, ssem, rsem, dev):
        return pltpu.make_async_remote_copy(
            src_ref=src, dst_ref=dst, send_sem=ssem, recv_sem=rsem, device_id=dev, device_id_type=MESH
        )

    def arrived(ref, sem):
        pltpu.make_async_copy(ref, ref, sem).wait()

    def slot(s, ff, tt):
        if s == 0:
            return WA.at[tt, pl.ds(pl.multiple_of(ff * ka, ka), ka)]
        if s == 1:
            return WO.at[ff, pl.ds(pl.multiple_of(tt * ko, ko), ko)]
        if s == 2:
            return WU.at[tt, pl.ds(pl.multiple_of(ff * ku, ku), ku)]
        if s == 3:
            return WD.at[ff, pl.ds(pl.multiple_of(tt * kd, kd), kd)]
        return table.at[ff, tt]

    def to_siblings(s, ff, src):
        for tt in siblings():
            copy(src, slot(s, ff, t), sd.at[s, ff], rd.at[s, ff], (r, f, tt)).start()

    def both_ways(s, ff, src):
        @pl.when(has_lo)
        def _():
            copy(src, slot(s, ff, t), sz.at[s, ff, 0], rz.at[s, ff], (r, f - 2, t)).start()

        @pl.when(has_hi)
        def _():
            copy(src, slot(s, ff, t), sz.at[s, ff, 1], rz.at[s, ff], (r, f + 2, t)).start()

    def fetches():
        for i, w in enumerate(weights):
            src, dst = weights[i], staged[i]
            if w.shape[1] > dst.shape[1]:
                n = dst.shape[1]
                src = src.at[:, pl.ds(pl.multiple_of(r * n, n), n)]
            elif w.shape[0] > dst.shape[0]:
                n = dst.shape[0]
                src = src.at[pl.ds(pl.multiple_of(r * n, n), n)]
            yield pltpu.make_async_copy(src, dst, loc.at[i])

    def round_stage(s):
        parts = {0: (0, 1, 2), 1: (3,), 2: (4,), 3: (5,)}[s]
        high = leaving[s].shape[0]
        for i in parts:
            pltpu.make_async_copy(staged[i], staged[i], loc.at[i]).wait()
        for yy in range(2):

            @pl.when(y == yy)
            def _():
                @pl.loop(0, high // 32)
                def _(k):
                    at = pl.ds(pl.multiple_of(k * 32, 32), 32)
                    for n, i in enumerate(parts):
                        if s in (0, 2):
                            wide = staged[i].shape[1] // 2
                            mine = staged[i][at, yy * wide : (yy + 1) * wide]
                            theirs = staged[i][at, (1 - yy) * wide : (2 - yy) * wide]
                        else:
                            wide = staged[i].shape[1]
                            mine = staged[i][pl.ds(pl.multiple_of(yy * high + k * 32, 32), 32), :]
                            theirs = staged[i][pl.ds(pl.multiple_of((1 - yy) * high + k * 32, 32), 32), :]
                        cols = slice(n * wide, (n + 1) * wide)
                        leaving[s][at, cols] = theirs.astype(bf16)
                        if s == 0:
                            WA[t, pl.ds(pl.multiple_of(f * ka + k * 32, 32), 32), cols] = mine.astype(bf16)
                        elif s == 1:
                            WO[f, pl.ds(pl.multiple_of(t * ko + k * 32, 32), 32), :] = mine.astype(bf16)
                        elif s == 2:
                            WU[t, pl.ds(pl.multiple_of(f * ku + k * 32, 32), 32), :] = mine.astype(bf16)
                        else:
                            WD[f, pl.ds(pl.multiple_of(t * kd + k * 32, 32), 32), :] = mine.astype(bf16)

    def kick(s):
        own = slot(s, f, t)
        copy(leaving[s] if s < 4 else own, own, sy.at[s], rz.at[s, f], (r, fy, t)).start()
        both_ways(s, f, own)
        to_siblings(s, f, own)

    def kick2(s):
        arrived(slot(s, fy, t), rz.at[s, fy])
        both_ways(s, fy, slot(s, fy, t))
        to_siblings(s, fy, slot(s, fy, t))

    def place(j):
        k = (j + 1) // 2
        sg = 1 - 2 * (j % 2)
        return z + sg * k, z - sg

    def step(s, j):
        zs, nxt = place(j)

        @pl.when(jnp.logical_and(zs >= 0, zs < nz))
        def _():
            for yy in range(2):
                ff = 2 * zs + yy
                arrived(slot(s, ff, t), rz.at[s, ff])

                @pl.when(jnp.logical_and(nxt >= 0, nxt < nz))
                def _():
                    copy(
                        slot(s, ff, t), slot(s, ff, t), sz.at[s, ff, 0], rz.at[s, ff], (r, 2 * nxt + y, t)
                    ).start()

                to_siblings(s, ff, slot(s, ff, t))

    def steps(s, lo, hi):
        @pl.loop(lo, hi)
        def _(j):
            step(s, j)

    def from_siblings(s, ff):
        for tt in siblings():
            arrived(slot(s, ff, tt), rd.at[s, ff])

    def all_from_siblings(s):
        @pl.loop(0, 2 * nz)
        def _(ff):
            from_siblings(s, ff)

    last = 2 * nz - 1

    for fetch in fetches():
        fetch.start()
    if inside:
        at_col = 0
        for v in vectors[:3]:
            packed[:, at_col : at_col + v.shape[1]] = v[...]
            at_col += v.shape[1]
        few = vectors[0].shape[1]
        for k in range(3):
            packed[:, at_col : at_col + few] = vectors[6][k : k + 1, pl.ds(pl.multiple_of(f * few, few), few)]
            at_col += few
        for v in vectors[3:6]:
            packed[:, at_col : at_col + v.shape[1]] = v[...]
            at_col += v.shape[1]
        table[f, t] = packed[...]

    barrier = pltpu.get_barrier_semaphore()
    for m in others():
        pl.semaphore_signal(barrier, inc=1, device_id=member(m), device_id_type=MESH)
    for tt in siblings():
        pl.semaphore_signal(barrier, inc=1, device_id=(r, f, tt), device_id_type=MESH)

    @pl.when(has_lo)
    def _():
        pl.semaphore_signal(barrier, inc=1, device_id=(r, f - 2, t), device_id_type=MESH)

    @pl.when(has_hi)
    def _():
        pl.semaphore_signal(barrier, inc=1, device_id=(r, f + 2, t), device_id_type=MESH)

    pl.semaphore_wait(barrier, G + T - 2 + (z + nz - 1) // nz + (2 * nz - 2 - z) // nz)

    round_stage(0)
    round_stage(1)
    kick(0)
    if inside:
        kick(4)
    kick(1)
    round_stage(2)
    round_stage(3)

    @pl.loop(0, win // TILE)
    def _(i):
        at = pl.ds(pl.multiple_of(i * TILE, TILE), TILE)
        x = tok[pl.ds(pl.multiple_of(start + i * TILE, TILE), TILE), :].astype(f32)
        x = x * lax.rsqrt(jnp.mean(x * x, axis=-1, keepdims=True) + norm_eps) * g1[...]
        nrm[g, at, :] = x.astype(bf16)

    kick2(0)
    if inside:
        kick2(4)
    for m in others():
        copy(nrm.at[g], nrm.at[g], sn.at[m], rn.at[g], member(m)).start()
    kick(2)
    kick2(1)
    steps(0, 1, last)
    if inside:
        steps(4, 1, last)
    kick(3)
    kick2(2)
    steps(1, 1, last)

    all_from_siblings(0)
    for m in others():
        arrived(nrm.at[m], rn.at[m])
    if inside:
        all_from_siblings(4)
        few, ups, outs = vectors[0].shape[1], vectors[3].shape[1], vectors[4].shape[1]
        wide = 3 * vectors[0].shape[1] * 2
        near = 2 * nz // G
        for tt in range(T):
            for j in range(near):
                row_of = table[g * near + j, tt]
                for k in range(3):
                    at_col = (k * near + j) * few
                    asc[tt, :, at_col : at_col + few] = row_of[:, k * few : (k + 1) * few]
                    taps[tt, k : k + 1, j * few : (j + 1) * few] = row_of[:, (3 + k) * few : (4 + k) * few]
                usc[tt, :, j * ups : (j + 1) * ups] = row_of[:, wide : wide + ups]
        for zs in range(nz):
            for yy in range(2):
                row_of = table[2 * zs + yy, 0]
                cols = slice(yy * outs, (yy + 1) * outs)
                oc[zs, :, cols] = row_of[:, wide + ups : wide + ups + outs]
                dc[zs, :, cols] = row_of[:, wide + ups + outs :]
    c = taps.shape[2]

    @pl.loop(0, G)
    def _(gs):
        x = nrm[gs]
        row = lax.broadcasted_iota(jnp.int32, (win, c), 0)
        for tt in range(T):
            prod = jnp.dot(x, WA[tt], preferred_element_type=f32) * asc[tt]
            gated = prod[:, c : 2 * c] * prod[:, :c]
            before = jnp.where(row == 0, 0.0, pltpu.roll(gated, 1, 0))
            after = jnp.where(row == win - 1, 0.0, pltpu.roll(gated, win - 1, 0))
            conv = taps[tt, 0:1] * before + taps[tt, 1:2] * gated + taps[tt, 2:3] * after
            hid[gs, :, tt * c : (tt + 1) * c] = (prod[:, 2 * c :] * conv).astype(bf16)

    all_from_siblings(1)

    @pl.loop(0, nz)
    def _(zs):
        @pl.loop(0, G)
        def _(gs):
            h = hid[gs, pl.ds(off, rows), :]
            for yy in range(2):
                p1[gs, zs, :, yy * cw : (yy + 1) * cw] = jnp.dot(
                    h, WO[2 * zs + yy], preferred_element_type=f32
                ).astype(bf16)

    kick2(3)
    for m in others():
        copy(p1.at[m], q1.at[g], s1.at[m], r1.at[g], member(m)).start()
    cut = (2 * last) // 3
    steps(2, 1, cut)

    for m in others():
        arrived(q1.at[m], r1.at[m])

    def total(p, q, zs, at):
        acc = p[g, zs, at, :].astype(f32)
        for m in others():
            acc = acc + q[m, zs, at, :].astype(f32)
        return acc

    @pl.loop(0, rows // TILE)
    def _(i):
        at = pl.ds(pl.multiple_of(i * TILE, TILE), TILE)
        here = pl.ds(pl.multiple_of(t * rows + i * TILE, TILE), TILE)
        ssq = jnp.zeros((TILE, 1), f32)
        for zs in range(nz):
            m = tok[here, zs * pw : (zs + 1) * pw].astype(f32) + total(p1, q1, zs, at) * oc[zs]
            mid32[zs, at, :] = m
            ssq = ssq + jnp.sum(m * m, axis=-1, keepdims=True)
        inv = lax.rsqrt(ssq / D + norm_eps)
        for zs in range(nz):
            cols = slice(zs * pw, (zs + 1) * pw)
            mid[g, at, cols] = (mid32[zs, at, :] * inv * g2[:, cols]).astype(bf16)

    steps(2, cut, cut + 1)
    for m in others():
        copy(mid.at[g], mid.at[g], sa.at[m], ra.at[g], member(m)).start()
    steps(2, cut + 1, last)
    cut2 = (last + 1) // 2
    steps(3, 1, cut2)

    all_from_siblings(2)
    for m in others():
        arrived(mid.at[m], ra.at[m])
    u = usc.shape[2]

    @pl.loop(0, G)
    def _(gs):
        x = mid[gs]
        for tt in range(T):
            upper = jnp.dot(x, WU[tt], preferred_element_type=f32) * usc[tt]
            act[gs, :, tt * u : (tt + 1) * u] = jnp.square(jnp.maximum(upper, 0.0)).astype(bf16)

    def down(j):
        zs, _ = place(j)

        @pl.when(jnp.logical_and(zs >= 0, zs < nz))
        def _():
            for yy in range(2):
                from_siblings(3, 2 * zs + yy)

            @pl.loop(0, G)
            def _(gs):
                x = act[gs]
                for yy in range(2):
                    p2[gs, zs, :, yy * cw : (yy + 1) * cw] = jnp.dot(
                        x, WD[2 * zs + yy], preferred_element_type=f32
                    ).astype(bf16)

            for m in others():
                copy(p2.at[m, zs], q2.at[g, zs], s2.at[m, zs], r2.at[g, zs], member(m)).start()

    @pl.loop(0, last)
    def _(j):
        @pl.when(j >= cut2)
        def _():
            step(3, j)

        down(j)

    @pl.loop(0, nz)
    def _(zs):
        for m in others():
            arrived(q2.at[m, zs], r2.at[m, zs])

    @pl.loop(0, rows // TILE)
    def _(i):
        at = pl.ds(pl.multiple_of(i * TILE, TILE), TILE)
        here = pl.ds(pl.multiple_of(t * rows + i * TILE, TILE), TILE)
        for zs in range(nz):
            out[here, zs * pw : (zs + 1) * pw] = (
                mid32[zs, at, :] + total(p2, q2, zs, at) * dc[zs]
            ).astype(bf16)

    def half(tt):
        return out.at[pl.ds(pl.multiple_of(tt * rows, rows), rows)]

    for tt in siblings():
        copy(half(t), half(t), so.at[tt], ro.at[t], (r, f, tt)).start()

    for s in stages:
        own = slot(s, f, t)
        arrived(own, sy.at[s])

        def gone(ff, k, s=s, own=own):
            arrived(own, sz.at[s, ff, k])

        for ff in (f, fy):
            pl.when(has_lo)(functools.partial(gone, ff, 0))
            pl.when(has_hi)(functools.partial(gone, ff, 1))

        @pl.loop(1, last)
        def _(j):
            zs, nxt = place(j)
            ok = jnp.logical_and(zs >= 0, zs < nz)

            @pl.when(jnp.logical_and(ok, jnp.logical_and(nxt >= 0, nxt < nz)))
            def _():
                for yy in range(2):
                    gone(2 * zs + yy, 0)

        @pl.loop(0, 2 * nz)
        def _(ff):
            for _ in siblings():
                arrived(own, sd.at[s, ff])

    for m in others():
        arrived(nrm.at[m], sn.at[m])
        arrived(p1.at[m], s1.at[m])
        arrived(mid.at[m], sa.at[m])

        @pl.loop(0, nz)
        def _(zs):
            arrived(p2.at[m, zs], s2.at[m, zs])

    for tt in siblings():
        arrived(half(tt), ro.at[tt])
        arrived(half(tt), so.at[tt])


def body(
    R, n_fs, T,
    tokens, mix_gain, value_weight, value_scale, inner_weight, inner_scale, outer_weight, outer_scale,
    conv_taps, out_weight, out_scale, mlp_gain, up_weight, up_scale, down_weight, down_scale,
):
    G, nz = 2 * R, n_fs // 2
    TOK, D = tokens.shape[1:]
    rows = TOK // T
    win = TOK if T == 1 else rows + HALO if T == 2 else rows + 2 * HALO
    r, f = lax.axis_index("rep"), lax.axis_index("fs")
    g = r * 2 + f % 2

    vs, us, os = value_scale.shape[0], up_scale.shape[0], out_scale.shape[0]
    inside = all(n % 128 == 0 for n in (vs, us, os))
    c, u = conv_taps.shape[1] // G, up_weight.shape[1] // G
    if inside:
        scales = (value_scale, inner_scale, outer_scale, up_scale, out_scale, down_scale)
        vectors = tuple(v[None] for v in scales) + (conv_taps,)
    else:
        tap = lax.dynamic_slice_in_dim(conv_taps, f * vs, vs, axis=1)
        packed = jnp.concatenate(
            [value_scale, inner_scale, outer_scale, tap[0], tap[1], tap[2], up_scale, out_scale, down_scale]
        )
        every = lax.all_gather(packed, ("tp", "fs"), axis=0, tiled=False).reshape(T, n_fs, -1)

        def block(v):
            return lax.dynamic_index_in_dim(v.reshape(T, G, -1), g, axis=1, keepdims=True)

        small = [block(every[:, :, i * vs : (i + 1) * vs]) for i in range(6)]
        asc = jnp.concatenate(small[:3], axis=2)
        taps = jnp.concatenate(small[3:], axis=1)
        usc = block(every[:, :, 6 * vs : 6 * vs + us])
        oc = every[0, :, 6 * vs + us : 6 * vs + us + os].reshape(nz, 1, -1)
        dc = every[0, :, 6 * vs + us + os :].reshape(nz, 1, -1)
        vectors = (asc, taps, usc, oc, dc)
    weights = (value_weight, inner_weight, outer_weight, out_weight, up_weight, down_weight)
    ka, ko, kd = value_weight.shape[0], out_weight.shape[0] // G, down_weight.shape[0] // G
    cw = out_weight.shape[1]
    rounded = [(ka, 3 * c), (ko, cw), (ka, u), (kd, cw)]
    staged = [(ka, 2 * c)] * 3 + [(2 * ko, cw), (ka, 2 * u), (2 * kd, cw)]
    gathered = ()
    if inside:
        L = 6 * vs + us + 2 * os
        small = [(1, L), (n_fs, T, 1, L), (T, 1, 3 * c), (T, 3, c), (T, 1, u), (nz, 1, 2 * cw), (nz, 1, 2 * cw)]
        gathered = tuple(pltpu.VMEM(shape, f32) for shape in small)
    pw = D // nz
    dma = pltpu.SemaphoreType.DMA
    vmem = pl.BlockSpec(memory_space=pltpu.VMEM)
    hbm = pl.BlockSpec(memory_space=pl.ANY)
    result = pl.pallas_call(
        functools.partial(kernel, nz, G, T, win, rows, inside),
        out_shape=jax.ShapeDtypeStruct((TOK, D), bf16),
        in_specs=[vmem] * 3 + [(vmem,) * len(vectors), (hbm,) * 6],
        out_specs=vmem,
        scratch_shapes=[
            pltpu.VMEM((T, D, 3 * c), bf16),
            pltpu.VMEM((n_fs, T * ko, cw), bf16),
            pltpu.VMEM((T, D, u), bf16),
            pltpu.VMEM((n_fs, T * kd, cw), bf16),
            pltpu.VMEM((G, win, D), bf16),
            pltpu.VMEM((G, win, T * ko), bf16),
            pltpu.VMEM((G, nz, rows, pw), bf16),
            pltpu.VMEM((G, nz, rows, pw), bf16),
            pltpu.VMEM((nz, rows, pw), f32),
            pltpu.VMEM((G, rows, D), bf16),
            pltpu.VMEM((G, rows, T * kd), bf16),
            pltpu.VMEM((G, nz, rows, pw), bf16),
            pltpu.VMEM((G, nz, rows, pw), bf16),
            tuple(pltpu.VMEM(shape, f32) for shape in staged),
            tuple(pltpu.VMEM(shape, bf16) for shape in rounded),
            gathered,
            dma((5, n_fs)),
            dma((5, n_fs)),
            dma((5, n_fs, 2)),
            dma((5, n_fs)),
            dma((5,)),
            dma((6,)),
            dma((G,)),
            dma((G,)),
            dma((G,)),
            dma((G,)),
            dma((G,)),
            dma((G,)),
            dma((G, nz)),
            dma((G, nz)),
            dma((T,)),
            dma((T,)),
        ],
        compiler_params=pltpu.CompilerParams(
            collective_id=0, has_side_effects=True, vmem_limit_bytes=65000000
        ),
    )(tokens[0], mix_gain[None], mlp_gain[None], vectors, weights)
    return result[None]


def solution(mesh):
    placed = (
        P(("rep", "fs"), None, None),
        P(),
        P("fs", "tp"),
        P(("tp", "fs")),
        P("fs", "tp"),
        P(("tp", "fs")),
        P("fs", "tp"),
        P(("tp", "fs")),
        P(None, "tp"),
        P("tp", "fs"),
        P("fs"),
        P(),
        P("fs", "tp"),
        P(("tp", "fs")),
        P("tp", "fs"),
        P("fs"),
    )
    sizes = (mesh.shape["rep"], mesh.shape["fs"], mesh.shape["tp"])
    return jax.shard_map(
        functools.partial(body, *sizes),
        mesh=mesh,
        in_specs=placed,
        out_specs=P(("rep", "fs"), None, None),
        check_vma=False,
    )
```

profile of v0, /device:TPU:0, one launch (start us, length us, event | category | flops | bytes accessed | tf_op | source)
XLA Modules:
  0.0 237.2 jit_solution(16701883263110110160)
XLA Ops:
  0.0 1.2 broadcast_in_dim.32.vectors_3_
  1.2 233.2 %shard_map.154 = bf16[384,2048]{1,0:T(8,128)(2,1)} custom-call(bf16[384,2048]{1,0:T(8,128)(2,1)} %bitcast.10, f32[1,2048]{1,0:T(1,128)} %bitcast.11, f32[1,2048]{1,0:T(1,128)} %bitcast.12, f32[1,128]{1,0:T(1,128)} %bitcast.15, f32[1,128]{1,0:T(1,128)} %bitcast.16, f32[1,128]{1,0:T(1,128)} %bitcast.17, f32[1,384]{1,0:T(1,128)} %broadcast_in_dim.32.vectors_3_, ...), custom_call_target="tpu_custom_call" | custom-call | tf_op jit(solution)/shard_map/pallas_call | solution.py:474
  234.4 2.7 %copy.18 = bf16[1,384,2048]{2,1,0:T(8,128)(2,1)} copy(bf16[1,384,2048]{2,1,0:T(8,128)(2,1)} %bitcast.9) | data formatting | bytes 3145728
where the time goes:
time: 237 us
  Pallas kernels  233 us (98%)
  local copies, waits for them, and re-layouts  3.97 us (2%)
    pallas_call x1, Pallas kernels, body(): pl.pallas_call(functools.partial(kernel, nz, G, T, win, rows, inside), ou...  233 us

commit v1 on v0

--- a/solution.py
+++ b/solution.py
@@ -13,7 +13,6 @@
 TILE = 16
 f32 = jnp.float32
 bf16 = jnp.bfloat16
-
 
 def kernel(
     nz, G, T, win, rows, inside,
@@ -421,6 +420,480 @@
         arrived(half(tt), ro.at[tt])
         arrived(half(tt), so.at[tt])
 
+def line_kernel(
+    nz, G, T, win, rows, inside,
+    tok, g1, g2, vectors, weights,
+    out,
+    WA, WO, WU, WD, nrm, hid, p1, q1, mid32, mid, act, p2, q2,
+    staged, leaving, gathered,
+    rz, rd, sz, sd, sy, loc, rn, sn, r1, s1, ra, sa, r2, s2, ro, so,
+):
+    if inside:
+        packed, table, asc, taps, usc, oc, dc = gathered
+    else:
+        asc, taps, usc, oc, dc = vectors
+    D = tok.shape[1]
+    pw = D // nz
+    cw = pw // 2
+    r, f, t = lax.axis_index("rep"), lax.axis_index("fs"), lax.axis_index("tp")
+    z, y = f // 2, f % 2
+    fy = z * 2 + 1 - y
+    g = r * 2 + y
+    ka, ko, ku, kd = (w.shape[0] for w in leaving)
+    stages = range(5 if inside else 4)
+    has_lo, has_hi = z > 0, z < nz - 1
+    outer = jnp.logical_or(z == 0, z == nz - 1)
+    inner = jnp.logical_not(outer)
+    inward = jnp.where(2 * z < nz, 1, -1)
+    across = z + 2 * inward
+    if T == 2:
+        start, off = t * (rows - HALO), t * HALO
+    else:
+        start = jnp.clip(t * rows - HALO, 0, tok.shape[0] - win)
+        off = t * rows - start
+    start, off = pl.multiple_of(start, HALO), pl.multiple_of(off, HALO)
+
+    def member(m):
+        return (m // 2, z * 2 + m % 2, t)
+
+    def others():
+        return [(g + d) % G for d in range(1, G)]
+
+    gx, gy, gd = (1 - r) * 2 + y, r * 2 + 1 - y, (1 - r) * 2 + 1 - y
+
+    def peers():
+        return [gd, gx, gy]
+
+    def siblings():
+        return [(t + d) % T for d in range(1, T)]
+
+    def copy(src, dst, ssem, rsem, dev):
+        return pltpu.make_async_remote_copy(
+            src_ref=src, dst_ref=dst, send_sem=ssem, recv_sem=rsem, device_id=dev, device_id_type=MESH
+        )
+
+    def arrived(ref, sem):
+        pltpu.make_async_copy(ref, ref, sem).wait()
+
+    def slot(s, ff, tt):
+        if s == 0:
+            return WA.at[tt, pl.ds(pl.multiple_of(ff * ka, ka), ka)]
+        if s == 1:
+            return WO.at[ff, pl.ds(pl.multiple_of(tt * ko, ko), ko)]
+        if s == 2:
+            return WU.at[tt, pl.ds(pl.multiple_of(ff * ku, ku), ku)]
+        if s == 3:
+            return WD.at[ff, pl.ds(pl.multiple_of(tt * kd, kd), kd)]
+        return table.at[ff, tt]
+
+    def to_siblings(s, ff, src):
+        for tt in siblings():
+            copy(src, slot(s, ff, t), sd.at[s, ff], rd.at[s, ff], (r, f, tt)).start()
+
+    def both_ways(s, ff, src):
+        @pl.when(has_lo)
+        def _():
+            copy(src, slot(s, ff, t), sz.at[s, ff, 0], rz.at[s, ff], (r, f - 2, t)).start()
+
+        @pl.when(has_hi)
+        def _():
+            copy(src, slot(s, ff, t), sz.at[s, ff, 1], rz.at[s, ff], (r, f + 2, t)).start()
+
+        @pl.when(outer)
+        def _():
+            copy(src, slot(s, ff, t), sz.at[s, ff, 2], rz.at[s, ff], (r, 2 * across + y, t)).start()
+
+    def fetches():
+        for i, w in enumerate(weights):
+            src, dst = weights[i], staged[i]
+            if w.shape[1] > dst.shape[1]:
+                n = dst.shape[1]
+                src = src.at[:, pl.ds(pl.multiple_of(r * n, n), n)]
+            elif w.shape[0] > dst.shape[0]:
+                n = dst.shape[0]
+                src = src.at[pl.ds(pl.multiple_of(r * n, n), n)]
+            yield pltpu.make_async_copy(src, dst, loc.at[i])
+
+    def round_stage(s):
+        parts = {0: (0, 1, 2), 1: (3,), 2: (4,), 3: (5,)}[s]
+        high = leaving[s].shape[0]
+        for i in parts:
+            pltpu.make_async_copy(staged[i], staged[i], loc.at[i]).wait()
+        for yy in range(2):
+
+            @pl.when(y == yy)
+            def _():
+                @pl.loop(0, high // 32)
+                def _(k):
+                    at = pl.ds(pl.multiple_of(k * 32, 32), 32)
+                    for n, i in enumerate(parts):
+                        if s in (0, 2):
+                            wide = staged[i].shape[1] // 2
+                            mine = staged[i][at, yy * wide : (yy + 1) * wide]
+                            theirs = staged[i][at, (1 - yy) * wide : (2 - yy) * wide]
+                        else:
+                            wide = staged[i].shape[1]
+                            mine = staged[i][pl.ds(pl.multiple_of(yy * high + k * 32, 32), 32), :]
+                            theirs = staged[i][pl.ds(pl.multiple_of((1 - yy) * high + k * 32, 32), 32), :]
+                        cols = slice(n * wide, (n + 1) * wide)
+                        leaving[s][at, cols] = theirs.astype(bf16)
+                        if s == 0:
+                            WA[t, pl.ds(pl.multiple_of(f * ka + k * 32, 32), 32), cols] = mine.astype(bf16)
+                        elif s == 1:
+                            WO[f, pl.ds(pl.multiple_of(t * ko + k * 32, 32), 32), :] = mine.astype(bf16)
+                        elif s == 2:
+                            WU[t, pl.ds(pl.multiple_of(f * ku + k * 32, 32), 32), :] = mine.astype(bf16)
+                        else:
+                            WD[f, pl.ds(pl.multiple_of(t * kd + k * 32, 32), 32), :] = mine.astype(bf16)
+
+    def swap(s):
+        own = slot(s, f, t)
+        copy(leaving[s] if s < 4 else own, own, sy.at[s], rz.at[s, f], (r, fy, t)).start()
+        to_siblings(s, f, own)
+
+    def spread(s):
+        both_ways(s, f, slot(s, f, t))
+
+    def kick2(s):
+        arrived(slot(s, fy, t), rz.at[s, fy])
+        both_ways(s, fy, slot(s, fy, t))
+        to_siblings(s, fy, slot(s, fy, t))
+
+    def place(j):
+        return (z + inward * j + nz) % nz
+
+    def relayed(zs):
+        return jnp.logical_and(inner, zs != z - inward)
+
+    blocks = 2 * (nz - 1)
+
+    def block(i):
+        first, rest = i < 2, jnp.maximum(i - 2, 0)
+        near_out, late_out = jnp.where(first, 1, 2 + rest % 2), jnp.where(first, i, rest // 2)
+        near_in, late_in = jnp.where(i < 4, 1 + i % 2, nz - 1), jnp.where(i < 4, i // 2, i % 2)
+        near, late = jnp.where(inner, near_in, near_out), jnp.where(inner, late_in, late_out)
+        return place(near), (y + late) % 2
+
+    def step(s, i):
+        zs, yy = block(i)
+        ff = 2 * zs + yy
+        arrived(slot(s, ff, t), rz.at[s, ff])
+
+        @pl.when(relayed(zs))
+        def _():
+            copy(
+                slot(s, ff, t), slot(s, ff, t), sz.at[s, ff, 0], rz.at[s, ff], (r, 2 * (z - inward) + y, t)
+            ).start()
+
+        to_siblings(s, ff, slot(s, ff, t))
+
+    def steps(s, lo, hi):
+        @pl.loop(lo, hi)
+        def _(j):
+            step(s, j)
+
+    def from_siblings(s, ff):
+        for tt in siblings():
+            arrived(slot(s, ff, tt), rd.at[s, ff])
+
+    def all_from_siblings(s):
+        @pl.loop(0, 2 * nz)
+        def _(ff):
+            from_siblings(s, ff)
+
+    for fetch in fetches():
+        fetch.start()
+    if inside:
+        at_col = 0
+        for v in vectors[:3]:
+            packed[:, at_col : at_col + v.shape[1]] = v[...]
+            at_col += v.shape[1]
+        few = vectors[0].shape[1]
+        for k in range(3):
+            packed[:, at_col : at_col + few] = vectors[6][k : k + 1, pl.ds(pl.multiple_of(f * few, few), few)]
+            at_col += few
+        for v in vectors[3:6]:
+            packed[:, at_col : at_col + v.shape[1]] = v[...]
+            at_col += v.shape[1]
+        table[f, t] = packed[...]
+
+    barrier = pltpu.get_barrier_semaphore()
+    for m in others():
+        pl.semaphore_signal(barrier, inc=1, device_id=member(m), device_id_type=MESH)
+    for tt in siblings():
+        pl.semaphore_signal(barrier, inc=1, device_id=(r, f, tt), device_id_type=MESH)
+
+    for zs in (z - 1, z + 1, across):
+        near = jnp.logical_and(zs >= 0, zs < nz)
+
+        @pl.when(jnp.logical_and(near, zs != z))
+        def _():
+            pl.semaphore_signal(barrier, inc=1, device_id=(r, 2 * zs + y, t), device_id_type=MESH)
+
+    pl.semaphore_wait(barrier, G + T - 2 + jnp.where(outer, 2, 3))
+
+    round_stage(0)
+    round_stage(1)
+    early = (0, 4, 1) if inside else (0, 1)
+    for s in early:
+        swap(s)
+        spread(s)
+    round_stage(2)
+    round_stage(3)
+
+    @pl.loop(0, win // TILE)
+    def _(i):
+        at = pl.ds(pl.multiple_of(i * TILE, TILE), TILE)
+        x = tok[pl.ds(pl.multiple_of(start + i * TILE, TILE), TILE), :].astype(f32)
+        x = x * lax.rsqrt(jnp.mean(x * x, axis=-1, keepdims=True) + norm_eps) * g1[...]
+        nrm[g, at, :] = x.astype(bf16)
+
+    for s in early:
+        kick2(s)
+    for m in (gx, gy):
+        copy(nrm.at[g], nrm.at[g], sn.at[m], rn.at[g], member(m)).start()
+    for s in (2, 3):
+        swap(s)
+
+    @pl.when(outer)
+    def _():
+        spread(2)
+        spread(3)
+
+    steps(0, 0, 2)
+
+    arrived(nrm.at[gy], rn.at[gy])
+    copy(nrm.at[gy], nrm.at[gy], sn.at[gd], rn.at[gy], member(gx)).start()
+
+    steps(0, 2, blocks)
+    if inside:
+        steps(4, 0, blocks)
+
+    @pl.when(inner)
+    def _():
+        spread(2)
+        kick2(2)
+
+    all_from_siblings(0)
+    if inside:
+        all_from_siblings(4)
+
+    for m in (gx, gd):
+        arrived(nrm.at[m], rn.at[m])
+    if inside:
+        few, ups, outs = vectors[0].shape[1], vectors[3].shape[1], vectors[4].shape[1]
+        wide = 3 * vectors[0].shape[1] * 2
+        near = 2 * nz // G
+        for tt in range(T):
+            for j in range(near):
+                row_of = table[g * near + j, tt]
+                for k in range(3):
+                    at_col = (k * near + j) * few
+                    asc[tt, :, at_col : at_col + few] = row_of[:, k * few : (k + 1) * few]
+                    taps[tt, k : k + 1, j * few : (j + 1) * few] = row_of[:, (3 + k) * few : (4 + k) * few]
+                usc[tt, :, j * ups : (j + 1) * ups] = row_of[:, wide : wide + ups]
+        for zs in range(nz):
+            for yy in range(2):
+                row_of = table[2 * zs + yy, 0]
+                cols = slice(yy * outs, (yy + 1) * outs)
+                oc[zs, :, cols] = row_of[:, wide + ups : wide + ups + outs]
+                dc[zs, :, cols] = row_of[:, wide + ups + outs :]
+    c = taps.shape[2]
+
+    @pl.loop(0, G)
+    def _(gs):
+        x = nrm[gs]
+        row = lax.broadcasted_iota(jnp.int32, (win, c), 0)
+        for tt in range(T):
+            prod = jnp.dot(x, WA[tt], preferred_element_type=f32) * asc[tt]
+            gated = prod[:, c : 2 * c] * prod[:, :c]
+            before = jnp.where(row == 0, 0.0, pltpu.roll(gated, 1, 0))
+            after = jnp.where(row == win - 1, 0.0, pltpu.roll(gated, win - 1, 0))
+            conv = taps[tt, 0:1] * before + taps[tt, 1:2] * gated + taps[tt, 2:3] * after
+            hid[gs, :, tt * c : (tt + 1) * c] = (prod[:, 2 * c :] * conv).astype(bf16)
+
+    @pl.loop(0, nz)
+    def _(j):
+        zs = place(j)
+
+        @pl.when(jnp.logical_and(j > 0, j < nz - 1))
+        def _():
+            steps(1, jnp.where(j == 1, 0, 3), jnp.where(j == 1, 3, blocks))
+
+        for yy in range(2):
+            from_siblings(1, 2 * zs + yy)
+
+        @pl.loop(0, G)
+        def _(gs):
+            h = hid[gs, pl.ds(off, rows), :]
+            for yy in range(2):
+                p1[gs, zs, :, yy * cw : (yy + 1) * cw] = jnp.dot(
+                    h, WO[2 * zs + yy], preferred_element_type=f32
+                ).astype(bf16)
+
+        for m in peers():
+            copy(p1.at[m, zs], q1.at[g, zs], s1.at[m, zs], r1.at[g, zs], member(m)).start()
+
+    @pl.when(outer)
+    def _():
+        kick2(2)
+        kick2(3)
+
+    cut = jnp.where(inner, blocks, 2)
+    steps(2, 0, cut)
+
+    @pl.when(inner)
+    def _():
+        spread(3)
+        kick2(3)
+
+    @pl.loop(0, nz)
+    def _(zs):
+        for m in others():
+            arrived(q1.at[m, zs], r1.at[m, zs])
+
+    def total(p, q, zs, at):
+        acc = p[g, zs, at, :].astype(f32)
+        for m in others():
+            acc = acc + q[m, zs, at, :].astype(f32)
+        return acc
+
+    @pl.loop(0, rows // TILE)
+    def _(i):
+        at = pl.ds(pl.multiple_of(i * TILE, TILE), TILE)
+        here = pl.ds(pl.multiple_of(t * rows + i * TILE, TILE), TILE)
+        ssq = jnp.zeros((TILE, 1), f32)
+        for zs in range(nz):
+            m = tok[here, zs * pw : (zs + 1) * pw].astype(f32) + total(p1, q1, zs, at) * oc[zs]
+            mid32[zs, at, :] = m
+            ssq = ssq + jnp.sum(m * m, axis=-1, keepdims=True)
+        inv = lax.rsqrt(ssq / D + norm_eps)
+        for zs in range(nz):
+            cols = slice(zs * pw, (zs + 1) * pw)
+            mid[g, at, cols] = (mid32[zs, at, :] * inv * g2[:, cols]).astype(bf16)
+
+    for m in (gx, gy):
+        copy(mid.at[g], mid.at[g], sa.at[m], ra.at[g], member(m)).start()
+
+    cut1 = jnp.where(inner, blocks, 4)
+    steps(2, cut, cut1)
+
+    part = rows // 2
+    for m, n, lo in ((gx, gy, part), (gy, gx, 0)):
+        arrived(mid.at[m], ra.at[m])
+        some = mid.at[m, pl.ds(lo, part)]
+        copy(some, some, sa.at[gd if lo else g], ra.at[m] if lo else ra.at[G], member(n)).start()
+
+    steps(2, cut1, blocks)
+
+    cut2 = jnp.where(inner, blocks, 0)
+    steps(3, 0, cut2)
+
+    all_from_siblings(2)
+
+    some = mid.at[gd, pl.ds(0, part)]
+    arrived(some, ra.at[gd])
+    arrived(some, ra.at[G])
+
+    u = usc.shape[2]
+
+    @pl.loop(0, G)
+    def _(gs):
+        x = mid[gs]
+        for tt in range(T):
+            upper = jnp.dot(x, WU[tt], preferred_element_type=f32) * usc[tt]
+            act[gs, :, tt * u : (tt + 1) * u] = jnp.square(jnp.maximum(upper, 0.0)).astype(bf16)
+
+    @pl.loop(0, nz)
+    def _(j):
+        zs = place(j)
+
+        @pl.when(outer & (j > 0) & (j < nz - 1))
+        def _():
+            steps(3, jnp.where(j == 1, 0, 2), jnp.where(j == 1, 2, blocks - 1))
+
+        @pl.when(outer & (j == nz - 1))
+        def _():
+            steps(3, blocks - 1, blocks)
+
+        for yy in range(2):
+            from_siblings(3, 2 * zs + yy)
+
+        @pl.loop(0, G)
+        def _(gs):
+            x = act[gs]
+            for yy in range(2):
+                p2[gs, zs, :, yy * cw : (yy + 1) * cw] = jnp.dot(
+                    x, WD[2 * zs + yy], preferred_element_type=f32
+                ).astype(bf16)
+
+        for m in peers():
+            copy(p2.at[m, zs], q2.at[g, zs], s2.at[m, zs], r2.at[g, zs], member(m)).start()
+
+    @pl.loop(0, nz)
+    def _(zs):
+        for m in others():
+            arrived(q2.at[m, zs], r2.at[m, zs])
+
+    @pl.loop(0, rows // TILE)
+    def _(i):
+        at = pl.ds(pl.multiple_of(i * TILE, TILE), TILE)
+        here = pl.ds(pl.multiple_of(t * rows + i * TILE, TILE), TILE)
+        for zs in range(nz):
+            out[here, zs * pw : (zs + 1) * pw] = (
+                mid32[zs, at, :] + total(p2, q2, zs, at) * dc[zs]
+            ).astype(bf16)
+
+    def half(tt):
+        return out.at[pl.ds(pl.multiple_of(tt * rows, rows), rows)]
+
+    for tt in siblings():
+        copy(half(t), half(t), so.at[tt], ro.at[t], (r, f, tt)).start()
+
+    for s in stages:
+        own = slot(s, f, t)
+        arrived(own, sy.at[s])
+
+        def gone(ff, k, s=s, own=own):
+            arrived(own, sz.at[s, ff, k])
+
+        for ff in (f, fy):
+            pl.when(has_lo)(functools.partial(gone, ff, 0))
+            pl.when(has_hi)(functools.partial(gone, ff, 1))
+            pl.when(outer)(functools.partial(gone, ff, 2))
+
+        @pl.loop(1, nz)
+        def _(j):
+            zs = place(j)
+
+            @pl.when(relayed(zs))
+            def _():
+                for yy in range(2):
+                    gone(2 * zs + yy, 0)
+
+        @pl.loop(0, 2 * nz)
+        def _(ff):
+            for _ in siblings():
+                arrived(own, sd.at[s, ff])
+
+    for m in others():
+        arrived(nrm.at[m], sn.at[m])
+
+    for m in (gx, gy):
+        arrived(mid.at[m], sa.at[m])
+    for m in (g, gd):
+        arrived(mid.at[g, pl.ds(0, part)], sa.at[m])
+
+    for m in others():
+
+        @pl.loop(0, nz)
+        def _(zs):
+            arrived(p1.at[m, zs], s1.at[m, zs])
+            arrived(p2.at[m, zs], s2.at[m, zs])
+
+    for tt in siblings():
+        arrived(half(tt), ro.at[tt])
+        arrived(half(tt), so.at[tt])
 
 def body(
     R, n_fs, T,
@@ -468,11 +941,12 @@
         small = [(1, L), (n_fs, T, 1, L), (T, 1, 3 * c), (T, 3, c), (T, 1, u), (nz, 1, 2 * cw), (nz, 1, 2 * cw)]
         gathered = tuple(pltpu.VMEM(shape, f32) for shape in small)
     pw = D // nz
+    lined = T == 2 and nz == 4 and R == 2
     dma = pltpu.SemaphoreType.DMA
     vmem = pl.BlockSpec(memory_space=pltpu.VMEM)
     hbm = pl.BlockSpec(memory_space=pl.ANY)
     result = pl.pallas_call(
-        functools.partial(kernel, nz, G, T, win, rows, inside),
+        functools.partial(line_kernel if lined else kernel, nz, G, T, win, rows, inside),
         out_shape=jax.ShapeDtypeStruct((TOK, D), bf16),
         in_specs=[vmem] * 3 + [(vmem,) * len(vectors), (hbm,) * 6],
         out_specs=vmem,
@@ -495,16 +969,16 @@
             gathered,
             dma((5, n_fs)),
             dma((5, n_fs)),
-            dma((5, n_fs, 2)),
+            dma((5, n_fs, 3)),
             dma((5, n_fs)),
             dma((5,)),
             dma((6,)),
             dma((G,)),
             dma((G,)),
-            dma((G,)),
-            dma((G,)),
-            dma((G,)),
-            dma((G,)),
+            dma((G, nz) if lined else (G,)),
+            dma((G, nz) if lined else (G,)),
+            dma((G + 1,)),
+            dma((G + 1,)),
             dma((G, nz)),
             dma((G, nz)),
             dma((T,)),
@@ -515,7 +989,6 @@
         ),
     )(tokens[0], mix_gain[None], mlp_gain[None], vectors, weights)
     return result[None]
-
 
 def solution(mesh):
     placed = (

time: 237 us -> 204 us (0.86)
  Pallas kernels: 233 us -> 200 us
    pallas_call x1, Pallas kernels: 233 us -> 200 us  [body(): pl.pallas_call(functools.partial(line_kernel if lined else kernel, nz, G,...]
where the time goes in v1:
time: 204 us
  Pallas kernels  200 us (98%)
  local copies, waits for them, and re-layouts  3.97 us (2%)
    pallas_call x1, Pallas kernels, body(): pl.pallas_call(functools.partial(line_kernel if lined else kernel, nz, G,...  200 us

profile of v1, /device:TPU:0, one launch (start us, length us, event | category | flops | bytes accessed | tf_op | source)
XLA Modules:
  0.0 204.2 jit_solution(18390570089028340522)
XLA Ops:
  0.0 1.2 broadcast_in_dim.32.vectors_3_
  1.2 200.2 %shard_map.154 = bf16[384,2048]{1,0:T(8,128)(2,1)} custom-call(bf16[384,2048]{1,0:T(8,128)(2,1)} %bitcast.10, f32[1,2048]{1,0:T(1,128)} %bitcast.11, f32[1,2048]{1,0:T(1,128)} %bitcast.12, f32[1,128]{1,0:T(1,128)} %bitcast.15, f32[1,128]{1,0:T(1,128)} %bitcast.16, f32[1,128]{1,0:T(1,128)} %bitcast.17, f32[1,384]{1,0:T(1,128)} %broadcast_in_dim.32.vectors_3_, ...), custom_call_target="tpu_custom_call" | custom-call | tf_op jit(solution)/shard_map/pallas_call | solution.py:948
  201.5 2.7 %copy.18 = bf16[1,384,2048]{2,1,0:T(8,128)(2,1)} copy(bf16[1,384,2048]{2,1,0:T(8,128)(2,1)} %bitcast.9) | data formatting | bytes 3145728

commit v2 on v1

--- a/solution.py
+++ b/solution.py
@@ -424,9 +424,9 @@
     nz, G, T, win, rows, inside,
     tok, g1, g2, vectors, weights,
     out,
-    WA, WO, WU, WD, nrm, hid, p1, q1, mid32, mid, act, p2, q2,
+    WA, WO, WU, WD, nrm, hid, p, q, mid32, mid, act,
     staged, leaving, gathered,
-    rz, rd, sz, sd, sy, loc, rn, sn, r1, s1, ra, sa, r2, s2, ro, so,
+    rz, rd, re, sz, sd, sy, loc, rn, sn, r1, s1, ra, sa, r2, s2, ro, so,
 ):
     if inside:
         packed, table, asc, taps, usc, oc, dc = gathered
@@ -488,20 +488,20 @@
 
     def to_siblings(s, ff, src):
         for tt in siblings():
-            copy(src, slot(s, ff, t), sd.at[s, ff], rd.at[s, ff], (r, f, tt)).start()
+            copy(src, slot(s, ff, t), sd.at[s], rd.at[s // 2, ff] if s % 2 else re.at[s // 2], (r, f, tt)).start()
 
     def both_ways(s, ff, src):
         @pl.when(has_lo)
         def _():
-            copy(src, slot(s, ff, t), sz.at[s, ff, 0], rz.at[s, ff], (r, f - 2, t)).start()
+            copy(src, slot(s, ff, t), sz.at[s], rz.at[s, ff], (r, f - 2, t)).start()
 
         @pl.when(has_hi)
         def _():
-            copy(src, slot(s, ff, t), sz.at[s, ff, 1], rz.at[s, ff], (r, f + 2, t)).start()
+            copy(src, slot(s, ff, t), sz.at[s], rz.at[s, ff], (r, f + 2, t)).start()
 
         @pl.when(outer)
         def _():
-            copy(src, slot(s, ff, t), sz.at[s, ff, 2], rz.at[s, ff], (r, 2 * across + y, t)).start()
+            copy(src, slot(s, ff, t), sz.at[s], rz.at[s, ff], (r, 2 * across + y, t)).start()
 
     def fetches():
         for i, w in enumerate(weights):
@@ -582,7 +582,7 @@
         @pl.when(relayed(zs))
         def _():
             copy(
-                slot(s, ff, t), slot(s, ff, t), sz.at[s, ff, 0], rz.at[s, ff], (r, 2 * (z - inward) + y, t)
+                slot(s, ff, t), slot(s, ff, t), sz.at[s], rz.at[s, ff], (r, 2 * (z - inward) + y, t)
             ).start()
 
         to_siblings(s, ff, slot(s, ff, t))
@@ -594,12 +594,22 @@
 
     def from_siblings(s, ff):
         for tt in siblings():
-            arrived(slot(s, ff, tt), rd.at[s, ff])
+            arrived(slot(s, ff, tt), rd.at[s // 2, ff])
+
+    def part_of(s, tt, n):
+        if s == 0:
+            return WA.at[tt, pl.ds(0, n * ka)]
+        if s == 1:
+            return WO.at[pl.ds(0, n), pl.ds(pl.multiple_of(tt * ko, ko), ko)]
+        if s == 2:
+            return WU.at[tt, pl.ds(0, n * ku)]
+        if s == 3:
+            return WD.at[pl.ds(0, n), pl.ds(pl.multiple_of(tt * kd, kd), kd)]
+        return table.at[pl.ds(0, n), tt]
 
     def all_from_siblings(s):
-        @pl.loop(0, 2 * nz)
-        def _(ff):
-            from_siblings(s, ff)
+        for tt in siblings():
+            arrived(part_of(s, tt, 2 * nz), re.at[s // 2])
 
     for fetch in fetches():
         fetch.start()
@@ -613,8 +623,9 @@
             packed[:, at_col : at_col + few] = vectors[6][k : k + 1, pl.ds(pl.multiple_of(f * few, few), few)]
             at_col += few
         for v in vectors[3:6]:
-            packed[:, at_col : at_col + v.shape[1]] = v[...]
-            at_col += v.shape[1]
+            for k in range(v.shape[0]):
+                packed[:, at_col : at_col + v.shape[1]] = v[k : k + 1, :]
+                at_col += v.shape[1]
         table[f, t] = packed[...]
 
     barrier = pltpu.get_barrier_semaphore()
@@ -630,10 +641,10 @@
         def _():
             pl.semaphore_signal(barrier, inc=1, device_id=(r, 2 * zs + y, t), device_id_type=MESH)
 
-    pl.semaphore_wait(barrier, G + T - 2 + jnp.where(outer, 2, 3))
-
     round_stage(0)
     round_stage(1)
+
+    pl.semaphore_wait(barrier, G + T - 2 + jnp.where(outer, 2, 3))
     early = (0, 4, 1) if inside else (0, 1)
     for s in early:
         swap(s)
@@ -651,26 +662,38 @@
     for s in early:
         kick2(s)
     for m in (gx, gy):
-        copy(nrm.at[g], nrm.at[g], sn.at[m], rn.at[g], member(m)).start()
+        copy(nrm.at[g], nrm.at[g], sn, rn.at[g], member(m)).start()
     for s in (2, 3):
         swap(s)
 
     @pl.when(outer)
     def _():
         spread(2)
+
+    steps(0, 0, 2)
+
+    arrived(nrm.at[gy], rn.at[gy])
+    copy(nrm.at[gy], nrm.at[gy], sn, rn.at[gy], member(gx)).start()
+
+    steps(0, 2, 4)
+
+    @pl.when(outer)
+    def _():
+        kick2(2)
         spread(3)
 
-    steps(0, 0, 2)
-
-    arrived(nrm.at[gy], rn.at[gy])
-    copy(nrm.at[gy], nrm.at[gy], sn.at[gd], rn.at[gy], member(gx)).start()
-
-    steps(0, 2, blocks)
+    steps(0, 4, blocks)
+
+    @pl.when(outer)
+    def _():
+        kick2(3)
+
     if inside:
         steps(4, 0, blocks)
 
     @pl.when(inner)
     def _():
+        steps(1, 0, blocks)
         spread(2)
         kick2(2)
 
@@ -681,7 +704,7 @@
     for m in (gx, gd):
         arrived(nrm.at[m], rn.at[m])
     if inside:
-        few, ups, outs = vectors[0].shape[1], vectors[3].shape[1], vectors[4].shape[1]
+        few, ups, outs = vectors[0].shape[1], vectors[3].size, vectors[4].shape[1]
         wide = 3 * vectors[0].shape[1] * 2
         near = 2 * nz // G
         for tt in range(T):
@@ -712,11 +735,18 @@
             conv = taps[tt, 0:1] * before + taps[tt, 1:2] * gated + taps[tt, 2:3] * after
             hid[gs, :, tt * c : (tt + 1) * c] = (prod[:, 2 * c :] * conv).astype(bf16)
 
+    def pair(ref, i, zs):
+        return ref.at[i, pl.ds(2 * zs, 2)]
+
+    def legs(zs):
+        even = zs % 2 == 0
+        return jnp.where(even, gx, gy), jnp.where(even, gy, gx)
+
     @pl.loop(0, nz)
     def _(j):
         zs = place(j)
 
-        @pl.when(jnp.logical_and(j > 0, j < nz - 1))
+        @pl.when(outer & (j > 0) & (j < nz - 1))
         def _():
             steps(1, jnp.where(j == 1, 0, 3), jnp.where(j == 1, 3, blocks))
 
@@ -727,17 +757,26 @@
         def _(gs):
             h = hid[gs, pl.ds(off, rows), :]
             for yy in range(2):
-                p1[gs, zs, :, yy * cw : (yy + 1) * cw] = jnp.dot(
-                    h, WO[2 * zs + yy], preferred_element_type=f32
-                ).astype(bf16)
-
-        for m in peers():
-            copy(p1.at[m, zs], q1.at[g, zs], s1.at[m, zs], r1.at[g, zs], member(m)).start()
-
-    @pl.when(outer)
-    def _():
-        kick2(2)
-        kick2(3)
+                p[gs, 2 * zs + yy] = jnp.dot(h, WO[2 * zs + yy], preferred_element_type=f32).astype(bf16)
+
+        first, _ = legs(zs)
+        copy(pair(p, gd, zs), pair(q, 1, zs), s1, r1.at[1, zs], member(first)).start()
+        copy(pair(p, first, zs), pair(q, 0, zs), s1, r1.at[0, zs], member(first)).start()
+
+    @pl.loop(0, nz)
+    def _(j):
+        zs = place(j)
+        _, second = legs(zs)
+        arrived(pair(q, 1, zs), r1.at[1, zs])
+
+        @pl.loop(0, rows // TILE)
+        def _(k):
+            at = pl.ds(pl.multiple_of(k * TILE, TILE), TILE)
+            for yy in range(2):
+                both = p[second, 2 * zs + yy, at, :].astype(f32) + q[1, 2 * zs + yy, at, :].astype(f32)
+                p[second, 2 * zs + yy, at, :] = both.astype(bf16)
+
+        copy(pair(p, second, zs), pair(q, 2, zs), s1, r1.at[2, zs], member(second)).start()
 
     cut = jnp.where(inner, blocks, 2)
     steps(2, 0, cut)
@@ -749,23 +788,19 @@
 
     @pl.loop(0, nz)
     def _(zs):
-        for m in others():
-            arrived(q1.at[m, zs], r1.at[m, zs])
-
-    def total(p, q, zs, at):
-        acc = p[g, zs, at, :].astype(f32)
-        for m in others():
-            acc = acc + q[m, zs, at, :].astype(f32)
-        return acc
+        for i in (0, 2):
+            arrived(pair(q, i, zs), r1.at[i, zs])
 
     @pl.loop(0, rows // TILE)
     def _(i):
         at = pl.ds(pl.multiple_of(i * TILE, TILE), TILE)
         here = pl.ds(pl.multiple_of(t * rows + i * TILE, TILE), TILE)
         ssq = jnp.zeros((TILE, 1), f32)
-        for zs in range(nz):
-            m = tok[here, zs * pw : (zs + 1) * pw].astype(f32) + total(p1, q1, zs, at) * oc[zs]
-            mid32[zs, at, :] = m
+        for ff in range(2 * nz):
+            half = slice(ff % 2 * cw, (ff % 2 + 1) * cw)
+            acc = p[g, ff, at, :].astype(f32) + q[0, ff, at, :].astype(f32) + q[2, ff, at, :].astype(f32)
+            m = tok[here, ff * cw : (ff + 1) * cw].astype(f32) + acc * oc[ff // 2, :, half]
+            mid32[ff // 2, at, half] = m
             ssq = ssq + jnp.sum(m * m, axis=-1, keepdims=True)
         inv = lax.rsqrt(ssq / D + norm_eps)
         for zs in range(nz):
@@ -773,7 +808,7 @@
             mid[g, at, cols] = (mid32[zs, at, :] * inv * g2[:, cols]).astype(bf16)
 
     for m in (gx, gy):
-        copy(mid.at[g], mid.at[g], sa.at[m], ra.at[g], member(m)).start()
+        copy(mid.at[g], mid.at[g], sa, ra.at[g], member(m)).start()
 
     cut1 = jnp.where(inner, blocks, 4)
     steps(2, cut, cut1)
@@ -782,7 +817,7 @@
     for m, n, lo in ((gx, gy, part), (gy, gx, 0)):
         arrived(mid.at[m], ra.at[m])
         some = mid.at[m, pl.ds(lo, part)]
-        copy(some, some, sa.at[gd if lo else g], ra.at[m] if lo else ra.at[G], member(n)).start()
+        copy(some, some, sa, ra.at[m] if lo else ra.at[G], member(n)).start()
 
     steps(2, cut1, blocks)
 
@@ -796,6 +831,7 @@
     arrived(some, ra.at[G])
 
     u = usc.shape[2]
+    arrived(p.at[pl.ds(0, G - 1)], s1)
 
     @pl.loop(0, G)
     def _(gs):
@@ -804,96 +840,74 @@
             upper = jnp.dot(x, WU[tt], preferred_element_type=f32) * usc[tt]
             act[gs, :, tt * u : (tt + 1) * u] = jnp.square(jnp.maximum(upper, 0.0)).astype(bf16)
 
-    @pl.loop(0, nz)
-    def _(j):
-        zs = place(j)
-
-        @pl.when(outer & (j > 0) & (j < nz - 1))
-        def _():
-            steps(3, jnp.where(j == 1, 0, 2), jnp.where(j == 1, 2, blocks - 1))
-
-        @pl.when(outer & (j == nz - 1))
-        def _():
-            steps(3, blocks - 1, blocks)
-
-        for yy in range(2):
-            from_siblings(3, 2 * zs + yy)
+    def source(i):
+        zs, yy = block(jnp.maximum(i - 2, 0))
+        zs, yy = jnp.where(i < 2, z, zs), jnp.where(i < 2, (y + i) % 2, yy)
+        return zs, yy, 2 * zs + yy
+
+    def finish(i):
+        zs, yy, ff = source(i)
+        for m in range(G - 1):
+            arrived(q.at[m, ff], r2.at[m, ff])
+        wide = pl.ds(pl.multiple_of(yy * cw, cw), cw)
+        cols = pl.ds(pl.multiple_of(ff * cw, cw), cw)
+
+        @pl.loop(0, rows // TILE)
+        def _(k):
+            at = pl.ds(pl.multiple_of(k * TILE, TILE), TILE)
+            acc = p[g, ff, at, :].astype(f32)
+            for m in range(G - 1):
+                acc = acc + q[m, ff, at, :].astype(f32)
+            here = pl.ds(pl.multiple_of(t * rows + k * TILE, TILE), TILE)
+            out[here, cols] = (mid32[zs, at, wide] + acc * dc[zs, :, wide]).astype(bf16)
+
+        mine = out.at[pl.ds(pl.multiple_of(t * rows, rows), rows), cols]
+        for tt in siblings():
+            copy(mine, mine, so, ro, (r, f, tt)).start()
+
+    @pl.loop(0, 2 * nz)
+    def _(ff_at):
+        _, _, ff = source(ff_at)
+
+        @pl.when(outer & (ff_at > 1))
+        def _():
+            step(3, ff_at - 2)
+
+        from_siblings(3, ff)
 
         @pl.loop(0, G)
         def _(gs):
-            x = act[gs]
-            for yy in range(2):
-                p2[gs, zs, :, yy * cw : (yy + 1) * cw] = jnp.dot(
-                    x, WD[2 * zs + yy], preferred_element_type=f32
-                ).astype(bf16)
-
-        for m in peers():
-            copy(p2.at[m, zs], q2.at[g, zs], s2.at[m, zs], r2.at[g, zs], member(m)).start()
-
-    @pl.loop(0, nz)
-    def _(zs):
-        for m in others():
-            arrived(q2.at[m, zs], r2.at[m, zs])
-
-    @pl.loop(0, rows // TILE)
+            p[gs, ff] = jnp.dot(act[gs], WD[ff], preferred_element_type=f32).astype(bf16)
+
+        for i, m in enumerate(peers()):
+            copy(p.at[m, ff], q.at[i, ff], s2, r2.at[i, ff], member(m)).start()
+
+        @pl.when(ff_at > 2)
+        def _():
+            finish(ff_at - 3)
+
+    @pl.loop(2 * nz - 3, 2 * nz)
     def _(i):
-        at = pl.ds(pl.multiple_of(i * TILE, TILE), TILE)
-        here = pl.ds(pl.multiple_of(t * rows + i * TILE, TILE), TILE)
-        for zs in range(nz):
-            out[here, zs * pw : (zs + 1) * pw] = (
-                mid32[zs, at, :] + total(p2, q2, zs, at) * dc[zs]
-            ).astype(bf16)
-
-    def half(tt):
-        return out.at[pl.ds(pl.multiple_of(tt * rows, rows), rows)]
-
-    for tt in siblings():
-        copy(half(t), half(t), so.at[tt], ro.at[t], (r, f, tt)).start()
+        finish(i)
 
     for s in stages:
-        own = slot(s, f, t)
-        arrived(own, sy.at[s])
-
-        def gone(ff, k, s=s, own=own):
-            arrived(own, sz.at[s, ff, k])
-
-        for ff in (f, fy):
-            pl.when(has_lo)(functools.partial(gone, ff, 0))
-            pl.when(has_hi)(functools.partial(gone, ff, 1))
-            pl.when(outer)(functools.partial(gone, ff, 2))
-
-        @pl.loop(1, nz)
-        def _(j):
-            zs = place(j)
-
-            @pl.when(relayed(zs))
-            def _():
-                for yy in range(2):
-                    gone(2 * zs + yy, 0)
-
-        @pl.loop(0, 2 * nz)
-        def _(ff):
-            for _ in siblings():
-                arrived(own, sd.at[s, ff])
-
-    for m in others():
-        arrived(nrm.at[m], sn.at[m])
-
-    for m in (gx, gy):
-        arrived(mid.at[m], sa.at[m])
-    for m in (g, gd):
-        arrived(mid.at[g, pl.ds(0, part)], sa.at[m])
-
-    for m in others():
-
-        @pl.loop(0, nz)
-        def _(zs):
-            arrived(p1.at[m, zs], s1.at[m, zs])
-            arrived(p2.at[m, zs], s2.at[m, zs])
-
-    for tt in siblings():
-        arrived(half(tt), ro.at[tt])
-        arrived(half(tt), so.at[tt])
+        arrived(slot(s, f, t), sy.at[s])
+        arrived(part_of(s, t, nz), sz.at[s])
+
+        @pl.when(inner)
+        def _():
+            arrived(part_of(s, t, nz), sz.at[s])
+
+        for _ in siblings():
+            arrived(part_of(s, t, 2 * nz), sd.at[s])
+
+    arrived(nrm.at[pl.ds(0, G - 1)], sn)
+    arrived(mid.at[pl.ds(0, G - 1)], sa)
+    arrived(p.at[pl.ds(0, G - 1)], s2)
+    half = out.at[pl.ds(0, rows)]
+    for _ in siblings():
+        arrived(half, ro)
+        arrived(half, so)
 
 def body(
     R, n_fs, T,
@@ -901,6 +915,7 @@
     conv_taps, out_weight, out_scale, mlp_gain, up_weight, up_scale, down_weight, down_scale,
 ):
     G, nz = 2 * R, n_fs // 2
+    lined = T == 2 and nz == 4 and R == 2
     TOK, D = tokens.shape[1:]
     rows = TOK // T
     win = TOK if T == 1 else rows + HALO if T == 2 else rows + 2 * HALO
@@ -912,7 +927,8 @@
     c, u = conv_taps.shape[1] // G, up_weight.shape[1] // G
     if inside:
         scales = (value_scale, inner_scale, outer_scale, up_scale, out_scale, down_scale)
-        vectors = tuple(v[None] for v in scales) + (conv_taps,)
+        wide = 128 if lined else us
+        vectors = tuple(v.reshape(-1, wide) if v is up_scale else v[None] for v in scales) + (conv_taps,)
     else:
         tap = lax.dynamic_slice_in_dim(conv_taps, f * vs, vs, axis=1)
         packed = jnp.concatenate(
@@ -941,22 +957,56 @@
         small = [(1, L), (n_fs, T, 1, L), (T, 1, 3 * c), (T, 3, c), (T, 1, u), (nz, 1, 2 * cw), (nz, 1, 2 * cw)]
         gathered = tuple(pltpu.VMEM(shape, f32) for shape in small)
     pw = D // nz
-    lined = T == 2 and nz == 4 and R == 2
     dma = pltpu.SemaphoreType.DMA
     vmem = pl.BlockSpec(memory_space=pltpu.VMEM)
     hbm = pl.BlockSpec(memory_space=pl.ANY)
-    result = pl.pallas_call(
-        functools.partial(line_kernel if lined else kernel, nz, G, T, win, rows, inside),
-        out_shape=jax.ShapeDtypeStruct((TOK, D), bf16),
-        in_specs=[vmem] * 3 + [(vmem,) * len(vectors), (hbm,) * 6],
-        out_specs=vmem,
-        scratch_shapes=[
-            pltpu.VMEM((T, D, 3 * c), bf16),
-            pltpu.VMEM((n_fs, T * ko, cw), bf16),
-            pltpu.VMEM((T, D, u), bf16),
-            pltpu.VMEM((n_fs, T * kd, cw), bf16),
-            pltpu.VMEM((G, win, D), bf16),
-            pltpu.VMEM((G, win, T * ko), bf16),
+    held = [
+        pltpu.VMEM((T, D, 3 * c), bf16),
+        pltpu.VMEM((n_fs, T * ko, cw), bf16),
+        pltpu.VMEM((T, D, u), bf16),
+        pltpu.VMEM((n_fs, T * kd, cw), bf16),
+        pltpu.VMEM((G, win, D), bf16),
+        pltpu.VMEM((G, win, T * ko), bf16),
+    ]
+    reading = [
+        tuple(pltpu.VMEM(shape, f32) for shape in staged),
+        tuple(pltpu.VMEM(shape, bf16) for shape in rounded),
+        gathered,
+    ]
+    if lined:
+        run = line_kernel
+        limit = 65000000
+        scratch = [
+            *held,
+            pltpu.VMEM((G, n_fs, rows, cw), bf16),
+            pltpu.VMEM((G - 1, n_fs, rows, cw), bf16),
+            pltpu.VMEM((nz, rows, pw), f32),
+            pltpu.VMEM((G, rows, D), bf16),
+            pltpu.VMEM((G, rows, T * kd), bf16),
+            *reading,
+            dma((5, n_fs)),
+            dma((2, n_fs)),
+            dma((3,)),
+            dma((5,)),
+            dma((5,)),
+            dma((5,)),
+            dma((6,)),
+            dma((G,)),
+            dma,
+            dma((G - 1, nz)),
+            dma,
+            dma((G + 1,)),
+            dma,
+            dma((G - 1, n_fs)),
+            dma,
+            dma,
+            dma,
+        ]
+    else:
+        run = kernel
+        limit = 65000000
+        scratch = [
+            *held,
             pltpu.VMEM((G, nz, rows, pw), bf16),
             pltpu.VMEM((G, nz, rows, pw), bf16),
             pltpu.VMEM((nz, rows, pw), f32),
@@ -964,29 +1014,31 @@
             pltpu.VMEM((G, rows, T * kd), bf16),
             pltpu.VMEM((G, nz, rows, pw), bf16),
             pltpu.VMEM((G, nz, rows, pw), bf16),
-            tuple(pltpu.VMEM(shape, f32) for shape in staged),
-            tuple(pltpu.VMEM(shape, bf16) for shape in rounded),
-            gathered,
+            *reading,
             dma((5, n_fs)),
             dma((5, n_fs)),
-            dma((5, n_fs, 3)),
+            dma((5, n_fs, 2)),
             dma((5, n_fs)),
             dma((5,)),
             dma((6,)),
             dma((G,)),
             dma((G,)),
-            dma((G, nz) if lined else (G,)),
-            dma((G, nz) if lined else (G,)),
-            dma((G + 1,)),
-            dma((G + 1,)),
+            dma((G,)),
+            dma((G,)),
+            dma((G,)),
+            dma((G,)),
             dma((G, nz)),
             dma((G, nz)),
             dma((T,)),
             dma((T,)),
-        ],
-        compiler_params=pltpu.CompilerParams(
-            collective_id=0, has_side_effects=True, vmem_limit_bytes=65000000
-        ),
+        ]
+    result = pl.pallas_call(
+        functools.partial(run, nz, G, T, win, rows, inside),
+        out_shape=jax.ShapeDtypeStruct((TOK, D), bf16),
+        in_specs=[vmem] * 3 + [(vmem,) * len(vectors), (hbm,) * 6],
+        out_specs=vmem,
+        scratch_shapes=scratch,
+        compiler_params=pltpu.CompilerParams(collective_id=0, has_side_effects=True, vmem_limit_bytes=limit),
     )(tokens[0], mix_gain[None], mlp_gain[None], vectors, weights)
     return result[None]
 

time: 204 us -> 192 us (0.941)
  Pallas kernels: 200 us -> 189 us
    pallas_call x1, Pallas kernels: 200 us -> 189 us  [body(): pl.pallas_call(functools.partial(run, nz, G, T, win, rows, inside), out_s...]
where the time goes in v2:
time: 192 us
  Pallas kernels  189 us (98%)
  local copies, waits for them, and re-layouts  2.73 us (1%)
    pallas_call x1, Pallas kernels, body(): pl.pallas_call(functools.partial(run, nz, G, T, win, rows, inside), out_s...  189 us

profile of v2, /device:TPU:0, one launch (start us, length us, event | category | flops | bytes accessed | tf_op | source)
XLA Modules:
  0.0 192.1 jit_solution(13073472811167458988)
XLA Ops:
  0.0 189.4 %shard_map.154 = bf16[384,2048]{1,0:T(8,128)(2,1)} custom-call(bf16[384,2048]{1,0:T(8,128)(2,1)} %bitcast.11, f32[1,2048]{1,0:T(1,128)} %bitcast.12, f32[1,2048]{1,0:T(1,128)} %bitcast.13, f32[1,128]{1,0:T(1,128)} %bitcast.17, f32[1,128]{1,0:T(1,128)} %bitcast.18, f32[1,128]{1,0:T(1,128)} %bitcast.19, f32[3,128]{1,0:T(4,128)} %bitcast.14, ...), custom_call_target="tpu_custom_call" | custom-call | tf_op jit(solution)/shard_map/pallas_call | solution.py:1035
  189.4 2.7 %copy.18 = bf16[1,384,2048]{2,1,0:T(8,128)(2,1)} copy(bf16[1,384,2048]{2,1,0:T(8,128)(2,1)} %bitcast.10) | data formatting | bytes 3145728

commit v3 on v2

--- a/solution.py
+++ b/solution.py
@@ -425,13 +425,10 @@
     tok, g1, g2, vectors, weights,
     out,
     WA, WO, WU, WD, nrm, hid, p, q, mid32, mid, act,
-    staged, leaving, gathered,
-    rz, rd, re, sz, sd, sy, loc, rn, sn, r1, s1, ra, sa, r2, s2, ro, so,
+    staged, leaving, gathered, detour,
+    rz, rd, re, sz, sd, sy, loc, rn, rb, rh, rt, sn, sh, st, r1, s1, ra, sa, r2, s2, ro, so,
 ):
-    if inside:
-        packed, table, asc, taps, usc, oc, dc = gathered
-    else:
-        asc, taps, usc, oc, dc = vectors
+    packed, table, asc, taps, usc, oc, dc = gathered
     D = tok.shape[1]
     pw = D // nz
     cw = pw // 2
@@ -440,8 +437,6 @@
     fy = z * 2 + 1 - y
     g = r * 2 + y
     ka, ko, ku, kd = (w.shape[0] for w in leaving)
-    stages = range(5 if inside else 4)
-    has_lo, has_hi = z > 0, z < nz - 1
     outer = jnp.logical_or(z == 0, z == nz - 1)
     inner = jnp.logical_not(outer)
     inward = jnp.where(2 * z < nz, 1, -1)
@@ -490,18 +485,26 @@
         for tt in siblings():
             copy(src, slot(s, ff, t), sd.at[s], rd.at[s // 2, ff] if s % 2 else re.at[s // 2], (r, f, tt)).start()
 
-    def both_ways(s, ff, src):
-        @pl.when(has_lo)
-        def _():
-            copy(src, slot(s, ff, t), sz.at[s], rz.at[s, ff], (r, f - 2, t)).start()
-
-        @pl.when(has_hi)
-        def _():
-            copy(src, slot(s, ff, t), sz.at[s], rz.at[s, ff], (r, f + 2, t)).start()
+    def send(s, ff, zs):
+        block = slot(s, ff, t)
+        copy(block, block, sz.at[s], rz.at[s, ff], (r, 2 * zs + y, t)).start()
+
+    def send_in(s, ff):
+        send(s, ff, z + inward)
+
+    def send_out(s, ff):
+        send(s, ff, z - inward)
+
+    def spread(s, ff):
+        send_in(s, ff)
+
+        @pl.when(inner)
+        def _():
+            send_out(s, ff)
 
         @pl.when(outer)
         def _():
-            copy(src, slot(s, ff, t), sz.at[s], rz.at[s, ff], (r, 2 * across + y, t)).start()
+            send(s, ff, across)
 
     def fetches():
         for i, w in enumerate(weights):
@@ -549,29 +552,23 @@
     def swap(s):
         own = slot(s, f, t)
         copy(leaving[s] if s < 4 else own, own, sy.at[s], rz.at[s, f], (r, fy, t)).start()
-        to_siblings(s, f, own)
-
-    def spread(s):
-        both_ways(s, f, slot(s, f, t))
-
-    def kick2(s):
+
+    def swapped(s):
         arrived(slot(s, fy, t), rz.at[s, fy])
-        both_ways(s, fy, slot(s, fy, t))
-        to_siblings(s, fy, slot(s, fy, t))
+
+    def both_to_siblings(s):
+        for ff in (f, fy):
+            to_siblings(s, ff, slot(s, ff, t))
 
     def place(j):
         return (z + inward * j + nz) % nz
 
-    def relayed(zs):
-        return jnp.logical_and(inner, zs != z - inward)
-
     blocks = 2 * (nz - 1)
 
     def block(i):
-        first, rest = i < 2, jnp.maximum(i - 2, 0)
-        near_out, late_out = jnp.where(first, 1, 2 + rest % 2), jnp.where(first, i, rest // 2)
-        near_in, late_in = jnp.where(i < 4, 1 + i % 2, nz - 1), jnp.where(i < 4, i // 2, i % 2)
-        near, late = jnp.where(inner, near_in, near_out), jnp.where(inner, late_in, late_out)
+        rest = jnp.maximum(i - 2, 0)
+        near_in, late_in = jnp.where(i < 2, 1, 2 + rest % 2), jnp.where(i < 2, i, rest // 2)
+        near, late = jnp.where(inner, near_in, 1 + i // 2), jnp.where(inner, late_in, i % 2)
         return place(near), (y + late) % 2
 
     def step(s, i):
@@ -579,12 +576,19 @@
         ff = 2 * zs + yy
         arrived(slot(s, ff, t), rz.at[s, ff])
 
-        @pl.when(relayed(zs))
-        def _():
-            copy(
-                slot(s, ff, t), slot(s, ff, t), sz.at[s], rz.at[s, ff], (r, 2 * (z - inward) + y, t)
-            ).start()
-
+        @pl.when(inner & (zs != z - inward))
+        def _():
+            send_out(s, ff)
+
+        to_siblings(s, ff, slot(s, ff, t))
+
+    def inner_step(s, near, late):
+        ff = 2 * place(near) + (y + late) % 2
+        arrived(slot(s, ff, t), rz.at[s, ff])
+        if s and near < nz - 1:
+            send_out(s, ff)
+        elif s == 0 and near == nz - 1:
+            send_in(0, ff)
         to_siblings(s, ff, slot(s, ff, t))
 
     def steps(s, lo, hi):
@@ -645,12 +649,25 @@
     round_stage(1)
 
     pl.semaphore_wait(barrier, G + T - 2 + jnp.where(outer, 2, 3))
-    early = (0, 4, 1) if inside else (0, 1)
-    for s in early:
-        swap(s)
-        spread(s)
+    swap(0)
+    send_in(0, f)
+    swap(4)
+    swap(1)
+
+    @pl.when(inner)
+    def _():
+        for s in (4, 1):
+            spread(s, f)
+
     round_stage(2)
     round_stage(3)
+
+    @pl.when(inner)
+    def _():
+        for s in (2, 3):
+            send_out(s, f)
+        for i in range(2):
+            copy(leaving[2 + i], detour[i], st.at[i], rt.at[i], (r, 2 * (z - inward) + y, t)).start()
 
     @pl.loop(0, win // TILE)
     def _(i):
@@ -659,51 +676,40 @@
         x = x * lax.rsqrt(jnp.mean(x * x, axis=-1, keepdims=True) + norm_eps) * g1[...]
         nrm[g, at, :] = x.astype(bf16)
 
-    for s in early:
-        kick2(s)
-    for m in (gx, gy):
-        copy(nrm.at[g], nrm.at[g], sn, rn.at[g], member(m)).start()
-    for s in (2, 3):
-        swap(s)
-
-    @pl.when(outer)
-    def _():
-        spread(2)
-
-    steps(0, 0, 2)
-
-    arrived(nrm.at[gy], rn.at[gy])
-    copy(nrm.at[gy], nrm.at[gy], sn, rn.at[gy], member(gx)).start()
-
-    steps(0, 2, 4)
-
-    @pl.when(outer)
-    def _():
-        kick2(2)
-        spread(3)
-
-    steps(0, 4, blocks)
-
-    @pl.when(outer)
-    def _():
-        kick2(3)
-
-    if inside:
-        steps(4, 0, blocks)
-
-    @pl.when(inner)
-    def _():
-        steps(1, 0, blocks)
-        spread(2)
-        kick2(2)
-
-    all_from_siblings(0)
-    if inside:
-        all_from_siblings(4)
-
-    for m in (gx, gd):
-        arrived(nrm.at[m], rn.at[m])
-    if inside:
+    low = win // 2 // TILE * TILE
+
+    def rows_of(i, lower):
+        return nrm.at[i, pl.ds(0, low)] if lower else nrm.at[i, pl.ds(low, win - low)]
+
+    def offer(base, sem):
+        for m in (gx, gy):
+            copy(nrm.at[base + g], nrm.at[base + g], sn, sem.at[g], member(m)).start()
+
+    def pass_on(base, sem, from_x):
+        m, n = (gx, gy) if from_x else (gy, gx)
+        arrived(nrm.at[base + m], sem.at[m])
+        some = rows_of(base + m, not from_x)
+        copy(some, some, sn, sem.at[m] if from_x else sem.at[G], member(n)).start()
+
+    def passed(base, sem):
+        arrived(rows_of(base + gd, False), sem.at[gd])
+        arrived(rows_of(base + gd, True), sem.at[G])
+
+    def project(base, gs):
+        x = nrm[base + gs]
+        row = lax.broadcasted_iota(jnp.int32, (win, c), 0)
+        for tt in range(T):
+            prod = jnp.dot(x, WA[tt], preferred_element_type=f32) * asc[tt]
+            gated = prod[:, c : 2 * c] * prod[:, :c]
+            before = jnp.where(row == 0, 0.0, pltpu.roll(gated, 1, 0))
+            after = jnp.where(row == win - 1, 0.0, pltpu.roll(gated, win - 1, 0))
+            conv = taps[tt, 0:1] * before + taps[tt, 1:2] * gated + taps[tt, 2:3] * after
+            hid[base + gs, :, tt * c : (tt + 1) * c] = (prod[:, 2 * c :] * conv).astype(bf16)
+
+    def nth(k):
+        return jnp.where(k == 0, g, jnp.where(k == 1, gx, jnp.where(k == 2, gy, gd)))
+
+    def unpack():
         few, ups, outs = vectors[0].shape[1], vectors[3].size, vectors[4].shape[1]
         wide = 3 * vectors[0].shape[1] * 2
         near = 2 * nz // G
@@ -723,17 +729,95 @@
                 dc[zs, :, cols] = row_of[:, wide + ups + outs :]
     c = taps.shape[2]
 
-    @pl.loop(0, G)
-    def _(gs):
-        x = nrm[gs]
-        row = lax.broadcasted_iota(jnp.int32, (win, c), 0)
-        for tt in range(T):
-            prod = jnp.dot(x, WA[tt], preferred_element_type=f32) * asc[tt]
-            gated = prod[:, c : 2 * c] * prod[:, :c]
-            before = jnp.where(row == 0, 0.0, pltpu.roll(gated, 1, 0))
-            after = jnp.where(row == win - 1, 0.0, pltpu.roll(gated, win - 1, 0))
-            conv = taps[tt, 0:1] * before + taps[tt, 1:2] * gated + taps[tt, 2:3] * after
-            hid[gs, :, tt * c : (tt + 1) * c] = (prod[:, 2 * c :] * conv).astype(bf16)
+    def project_far(lo, hi):
+        @pl.loop(lo, hi)
+        def _(k):
+            gs = nth(k)
+
+            @pl.when(k == G - 1)
+            def _():
+                passed(G, rb)
+
+            project(G, gs)
+            here = pl.ds(off, rows)
+            copy(hid.at[G + gs, here], hid.at[gs, here], sh, rh.at[gs], (r, 2 * (z - inward) + y, t)).start()
+
+    @pl.when(outer)
+    def _():
+        swap(2)
+        swap(3)
+        spread(4, f)
+        swapped(0)
+        send_in(0, fy)
+        swapped(4)
+        spread(4, fy)
+        copy(nrm.at[g], nrm.at[G + g], sn, rb.at[g], (r, 2 * (z + inward) + y, t)).start()
+        spread(1, f)
+        swapped(1)
+        spread(1, fy)
+        for s in (4, 1):
+            both_to_siblings(s)
+        spread(2, f)
+        for i in range(2):
+            arrived(detour[i], rt.at[i])
+            ff = 2 * (z + inward) + y
+            copy(detour[i], slot(2 + i, ff, t), st.at[i], rz.at[2 + i, ff], (r, fy, t)).start()
+        def give_back(i):
+            ff = 2 * (z + inward) + 1 - y
+            arrived(slot(2 + i, ff, t), rz.at[2 + i, ff])
+            send_in(2 + i, ff)
+            to_siblings(2 + i, ff, slot(2 + i, ff, t))
+
+        give_back(0)
+        swapped(2)
+        spread(2, fy)
+        both_to_siblings(2)
+        give_back(1)
+        swapped(3)
+        for ff in (f, fy):
+            spread(3, ff)
+        both_to_siblings(3)
+        steps(4, 0, blocks)
+        steps(1, 0, blocks)
+        all_from_siblings(4)
+        unpack()
+
+    @pl.when(inner)
+    def _():
+        offer(0, rn)
+        swapped(0)
+        send_in(0, fy)
+        both_to_siblings(0)
+        inner_step(0, 3, 0)
+        inner_step(0, 1, 0)
+        for s in (4, 1):
+            swapped(s)
+            spread(s, fy)
+            both_to_siblings(s)
+        pass_on(0, rn, True)
+        inner_step(0, 2, 0)
+        inner_step(0, 1, 1)
+        pass_on(0, rn, False)
+        inner_step(0, 3, 1)
+        arrived(nrm.at[G + g], rb.at[g])
+        offer(G, rb)
+        inner_step(0, 2, 1)
+        for s in (2, 3):
+            send_in(s, f)
+        all_from_siblings(0)
+        steps(4, 0, blocks)
+        all_from_siblings(4)
+        unpack()
+        steps(1, 0, blocks)
+        passed(0, rn)
+        @pl.loop(0, G)
+        def _(gs):
+            project(0, gs)
+    @pl.when(inner)
+    def _():
+        project_far(0, 1)
+        pass_on(G, rb, True)
+        pass_on(G, rb, False)
 
     def pair(ref, i, zs):
         return ref.at[i, pl.ds(2 * zs, 2)]
@@ -742,26 +826,56 @@
         even = zs % 2 == 0
         return jnp.where(even, gx, gy), jnp.where(even, gy, gx)
 
-    @pl.loop(0, nz)
-    def _(j):
-        zs = place(j)
-
-        @pl.when(outer & (j > 0) & (j < nz - 1))
-        def _():
-            steps(1, jnp.where(j == 1, 0, 3), jnp.where(j == 1, 3, blocks))
-
-        for yy in range(2):
-            from_siblings(1, 2 * zs + yy)
-
-        @pl.loop(0, G)
-        def _(gs):
-            h = hid[gs, pl.ds(off, rows), :]
-            for yy in range(2):
-                p[gs, 2 * zs + yy] = jnp.dot(h, WO[2 * zs + yy], preferred_element_type=f32).astype(bf16)
-
+    def first_leg(zs):
         first, _ = legs(zs)
         copy(pair(p, gd, zs), pair(q, 1, zs), s1, r1.at[1, zs], member(first)).start()
         copy(pair(p, first, zs), pair(q, 0, zs), s1, r1.at[0, zs], member(first)).start()
+
+    def own_leg(j, k):
+        zs = 2 * j + k
+        first, _ = legs(zs)
+        copy(pair(p, first, zs), pair(q, 0, zs), s1, r1.at[0, zs], member(first)).start()
+
+    def pass_leg(zs):
+        first, _ = legs(zs)
+        copy(pair(p, gd, zs), pair(q, 1, zs), s1, r1.at[1, zs], member(first)).start()
+
+    pl.when(inner)(lambda: project_far(1, 3))
+
+    @pl.loop(0, 2 * nz)
+    def _(ff):
+        from_siblings(1, ff)
+
+    @pl.loop(0, G)
+    def _(k):
+        gs = nth(k)
+
+        @pl.when(outer)
+        def _():
+            some = hid.at[gs, pl.ds(off, rows)]
+            arrived(some, rh.at[gs])
+
+        @pl.loop(0, 2 * nz)
+        def _(ff):
+            h = hid[gs, pl.ds(off, rows), :]
+            p[gs, ff] = jnp.dot(h, WO[ff], preferred_element_type=f32).astype(bf16)
+
+        @pl.when(outer & (k > 0) & (k < G - 1))
+        def _():
+            pl.loop(0, nz // 2)(lambda j: own_leg(j, k - 1))
+
+        @pl.when(outer & (k == G - 1))
+        def _():
+            pl.loop(0, nz)(pass_leg)
+
+    @pl.when(inner)
+    def _():
+        pl.loop(0, nz)(pass_leg)
+        for k in range(2):
+            pl.loop(0, nz // 2)(lambda j: own_leg(j, k))
+        project_far(3, G)
+        inner_step(2, 1, 0)
+        inner_step(2, 2, 0)
 
     @pl.loop(0, nz)
     def _(j):
@@ -778,13 +892,13 @@
 
         copy(pair(p, second, zs), pair(q, 2, zs), s1, r1.at[2, zs], member(second)).start()
 
-    cut = jnp.where(inner, blocks, 2)
-    steps(2, 0, cut)
-
     @pl.when(inner)
     def _():
-        spread(3)
-        kick2(3)
+        swapped(2)
+        send_in(2, fy)
+        both_to_siblings(2)
+
+    pl.when(outer)(lambda: steps(2, 0, 1))
 
     @pl.loop(0, nz)
     def _(zs):
@@ -810,8 +924,15 @@
     for m in (gx, gy):
         copy(mid.at[g], mid.at[g], sa, ra.at[g], member(m)).start()
 
-    cut1 = jnp.where(inner, blocks, 4)
-    steps(2, cut, cut1)
+    pl.when(outer)(lambda: steps(2, 2, 4))
+
+    @pl.when(inner)
+    def _():
+        inner_step(2, 2, 1)
+        swapped(3)
+        send_in(3, fy)
+        both_to_siblings(3)
+        inner_step(2, 1, 1)
 
     part = rows // 2
     for m, n, lo in ((gx, gy, part), (gy, gx, 0)):
@@ -819,48 +940,81 @@
         some = mid.at[m, pl.ds(lo, part)]
         copy(some, some, sa, ra.at[m] if lo else ra.at[G], member(n)).start()
 
-    steps(2, cut1, blocks)
-
-    cut2 = jnp.where(inner, blocks, 0)
-    steps(3, 0, cut2)
+    pl.when(outer)(lambda: steps(2, 4, blocks))
+
+    @pl.when(inner)
+    def _():
+        inner_step(3, 1, 0)
+        inner_step(2, 3, 0)
+        inner_step(2, 3, 1)
 
     all_from_siblings(2)
-
-    some = mid.at[gd, pl.ds(0, part)]
-    arrived(some, ra.at[gd])
-    arrived(some, ra.at[G])
-
     u = usc.shape[2]
     arrived(p.at[pl.ds(0, G - 1)], s1)
 
     @pl.loop(0, G)
-    def _(gs):
+    def _(k):
+        gs = nth(k)
+
+        @pl.when(k == G - 1)
+        def _():
+            some = mid.at[gd, pl.ds(0, part)]
+            arrived(some, ra.at[gd])
+            arrived(some, ra.at[G])
+
         x = mid[gs]
         for tt in range(T):
             upper = jnp.dot(x, WU[tt], preferred_element_type=f32) * usc[tt]
             act[gs, :, tt * u : (tt + 1) * u] = jnp.square(jnp.maximum(upper, 0.0)).astype(bf16)
 
+    pl.when(inner)(lambda: inner_step(3, 1, 1))
+
     def source(i):
         zs, yy = block(jnp.maximum(i - 2, 0))
         zs, yy = jnp.where(i < 2, z, zs), jnp.where(i < 2, (y + i) % 2, yy)
         return zs, yy, 2 * zs + yy
 
+    def direct(i):
+        zs, _, _ = source(i)
+        return outer & (zs == place(nz - 1))
+
+    def second_leg(i):
+        _, _, ff = source(i)
+        _, second = legs(ff)
+
+        @pl.when(jnp.logical_not(direct(i)))
+        def _():
+            arrived(q.at[1, ff], r2.at[1, ff])
+
+            @pl.loop(0, rows // TILE)
+            def _(k):
+                at = pl.ds(pl.multiple_of(k * TILE, TILE), TILE)
+                both = p[second, ff, at, :].astype(f32) + q[1, ff, at, :].astype(f32)
+                p[second, ff, at, :] = both.astype(bf16)
+
+            copy(p.at[second, ff], q.at[2, ff], s2, r2.at[2, ff], member(second)).start()
+
     def finish(i):
         zs, yy, ff = source(i)
-        for m in range(G - 1):
-            arrived(q.at[m, ff], r2.at[m, ff])
         wide = pl.ds(pl.multiple_of(yy * cw, cw), cw)
         cols = pl.ds(pl.multiple_of(ff * cw, cw), cw)
 
-        @pl.loop(0, rows // TILE)
-        def _(k):
-            at = pl.ds(pl.multiple_of(k * TILE, TILE), TILE)
-            acc = p[g, ff, at, :].astype(f32)
-            for m in range(G - 1):
-                acc = acc + q[m, ff, at, :].astype(f32)
-            here = pl.ds(pl.multiple_of(t * rows + k * TILE, TILE), TILE)
-            out[here, cols] = (mid32[zs, at, wide] + acc * dc[zs, :, wide]).astype(bf16)
-
+        def sum_up(slots):
+            for m in slots:
+                arrived(q.at[m, ff], r2.at[m, ff])
+
+            @pl.loop(0, rows // TILE)
+            def _(k):
+                at = pl.ds(pl.multiple_of(k * TILE, TILE), TILE)
+                acc = p[g, ff, at, :].astype(f32)
+                for m in slots:
+                    acc = acc + q[m, ff, at, :].astype(f32)
+                here = pl.ds(pl.multiple_of(t * rows + k * TILE, TILE), TILE)
+                out[here, cols] = (mid32[zs, at, wide] + acc * dc[zs, :, wide]).astype(bf16)
+
+        far = direct(i)
+        pl.when(far)(lambda: sum_up((0, 1, 2)))
+        pl.when(jnp.logical_not(far))(lambda: sum_up((0, 2)))
         mine = out.at[pl.ds(pl.multiple_of(t * rows, rows), rows), cols]
         for tt in siblings():
             copy(mine, mine, so, ro, (r, f, tt)).start()
@@ -869,9 +1023,12 @@
     def _(ff_at):
         _, _, ff = source(ff_at)
 
-        @pl.when(outer & (ff_at > 1))
+        @pl.when(outer & (ff_at > 1) & (ff_at != 3))
         def _():
             step(3, ff_at - 2)
+
+        for i, (near, late) in enumerate(((2, 0), (3, 0), (2, 1), (3, 1))):
+            pl.when(inner & (ff_at == 4 + i))(functools.partial(inner_step, 3, near, late))
 
         from_siblings(3, ff)
 
@@ -879,29 +1036,67 @@
         def _(gs):
             p[gs, ff] = jnp.dot(act[gs], WD[ff], preferred_element_type=f32).astype(bf16)
 
-        for i, m in enumerate(peers()):
-            copy(p.at[m, ff], q.at[i, ff], s2, r2.at[i, ff], member(m)).start()
-
-        @pl.when(ff_at > 2)
-        def _():
-            finish(ff_at - 3)
-
-    @pl.loop(2 * nz - 3, 2 * nz)
+        first, second = legs(ff)
+        far = direct(ff_at)
+        copy(p.at[gd, ff], q.at[1, ff], s2, r2.at[1, ff], member(jnp.where(far, gd, first))).start()
+        copy(p.at[first, ff], q.at[0, ff], s2, r2.at[0, ff], member(first)).start()
+
+        @pl.when(far)
+        def _():
+            copy(p.at[second, ff], q.at[2, ff], s2, r2.at[2, ff], member(second)).start()
+
+        @pl.when(ff_at > 1)
+        def _():
+            second_leg(ff_at - 2)
+
+        @pl.when(ff_at > 3)
+        def _():
+            finish(ff_at - 4)
+
+    @pl.loop(2 * nz - 2, 2 * nz)
+    def _(i):
+        second_leg(i)
+        finish(i - 2)
+
+    @pl.loop(2 * nz - 2, 2 * nz)
     def _(i):
         finish(i)
 
-    for s in stages:
-        arrived(slot(s, f, t), sy.at[s])
-        arrived(part_of(s, t, nz), sz.at[s])
+    for s in range(5):
+        if s in (2, 3):
+            pl.when(outer)(functools.partial(arrived, slot(s, f, t), sy.at[s]))
+        else:
+            arrived(slot(s, f, t), sy.at[s])
+        few_sent, many_sent = {0: (2, 4), 2: (5, 7), 3: (5, 7)}.get(s, (4, 8))
+
+        @pl.when(outer)
+        def _():
+            arrived(part_of(s, t, few_sent), sz.at[s])
 
         @pl.when(inner)
         def _():
-            arrived(part_of(s, t, nz), sz.at[s])
-
-        for _ in siblings():
-            arrived(part_of(s, t, 2 * nz), sd.at[s])
-
-    arrived(nrm.at[pl.ds(0, G - 1)], sn)
+            arrived(part_of(s, t, many_sent), sz.at[s])
+
+        def gone(s=s):
+            for _ in siblings():
+                arrived(part_of(s, t, 2 * nz), sd.at[s])
+
+        if s == 0:
+            pl.when(inner)(gone)
+        else:
+            gone()
+
+    @pl.when(outer)
+    def _():
+        arrived(nrm.at[0], sn)
+
+    @pl.when(inner)
+    def _():
+        arrived(nrm.at[pl.ds(0, 2 * (G - 1))], sn)
+        arrived(hid.at[pl.ds(0, G), pl.ds(0, rows)], sh)
+
+    for i in range(2):
+        arrived(detour[i], st.at[i])
     arrived(mid.at[pl.ds(0, G - 1)], sa)
     arrived(p.at[pl.ds(0, G - 1)], s2)
     half = out.at[pl.ds(0, rows)]
@@ -915,7 +1110,6 @@
     conv_taps, out_weight, out_scale, mlp_gain, up_weight, up_scale, down_weight, down_scale,
 ):
     G, nz = 2 * R, n_fs // 2
-    lined = T == 2 and nz == 4 and R == 2
     TOK, D = tokens.shape[1:]
     rows = TOK // T
     win = TOK if T == 1 else rows + HALO if T == 2 else rows + 2 * HALO
@@ -924,6 +1118,7 @@
 
     vs, us, os = value_scale.shape[0], up_scale.shape[0], out_scale.shape[0]
     inside = all(n % 128 == 0 for n in (vs, us, os))
+    lined = inside and T == 2 and nz == 4 and R == 2
     c, u = conv_taps.shape[1] // G, up_weight.shape[1] // G
     if inside:
         scales = (value_scale, inner_scale, outer_scale, up_scale, out_scale, down_scale)
@@ -965,8 +1160,8 @@
         pltpu.VMEM((n_fs, T * ko, cw), bf16),
         pltpu.VMEM((T, D, u), bf16),
         pltpu.VMEM((n_fs, T * kd, cw), bf16),
-        pltpu.VMEM((G, win, D), bf16),
-        pltpu.VMEM((G, win, T * ko), bf16),
+        pltpu.VMEM((2 * G if lined else G, win, D), bf16),
+        pltpu.VMEM((2 * G if lined else G, win, T * ko), bf16),
     ]
     reading = [
         tuple(pltpu.VMEM(shape, f32) for shape in staged),
@@ -984,6 +1179,7 @@
             pltpu.VMEM((G, rows, D), bf16),
             pltpu.VMEM((G, rows, T * kd), bf16),
             *reading,
+            tuple(pltpu.VMEM(shape, bf16) for shape in rounded[2:]),
             dma((5, n_fs)),
             dma((2, n_fs)),
             dma((3,)),
@@ -991,8 +1187,13 @@
             dma((5,)),
             dma((5,)),
             dma((6,)),
+            dma((G + 1,)),
+            dma((G + 1,)),
             dma((G,)),
+            dma((2,)),
             dma,
+            dma,
+            dma((2,)),
             dma((G - 1, nz)),
             dma,
             dma((G + 1,)),

time: 192 us -> 177 us (0.922)
  Pallas kernels: 189 us -> 173 us
    pallas_call x1, Pallas kernels: 189 us -> 173 us  [body(): pl.pallas_call(functools.partial(run, nz, G, T, win, rows, inside), out_s...]
where the time goes in v3:
time: 177 us; the launch traced here: 176 us
  Pallas kernels  173 us (98%)
  local copies, waits for them, and re-layouts  2.73 us (2%)
    pallas_call x1, Pallas kernels, body(): pl.pallas_call(functools.partial(run, nz, G, T, win, rows, inside), out_s...  173 us

profile of v3, /device:TPU:0, one launch (start us, length us, event | category | flops | bytes accessed | tf_op | source)
XLA Modules:
  0.0 175.7 jit_solution(7681438146836642090)
XLA Ops:
  0.0 173.0 %shard_map.154 = bf16[384,2048]{1,0:T(8,128)(2,1)} custom-call(bf16[384,2048]{1,0:T(8,128)(2,1)} %bitcast.11, f32[1,2048]{1,0:T(1,128)} %bitcast.12, f32[1,2048]{1,0:T(1,128)} %bitcast.13, f32[1,128]{1,0:T(1,128)} %bitcast.17, f32[1,128]{1,0:T(1,128)} %bitcast.18, f32[1,128]{1,0:T(1,128)} %bitcast.19, f32[3,128]{1,0:T(4,128)} %bitcast.14, ...), custom_call_target="tpu_custom_call" | custom-call | tf_op jit(solution)/shard_map/pallas_call | solution.py:1236
  173.0 2.7 %copy.18 = bf16[1,384,2048]{2,1,0:T(8,128)(2,1)} copy(bf16[1,384,2048]{2,1,0:T(8,128)(2,1)} %bitcast.10) | data formatting | bytes 3145728

commit v4 on v3

--- a/solution.py
+++ b/solution.py
@@ -13,6 +13,7 @@
 TILE = 16
 f32 = jnp.float32
 bf16 = jnp.bfloat16
+
 
 def kernel(
     nz, G, T, win, rows, inside,
@@ -420,13 +421,14 @@
         arrived(half(tt), ro.at[tt])
         arrived(half(tt), so.at[tt])
 
+
 def line_kernel(
     nz, G, T, win, rows, inside,
     tok, g1, g2, vectors, weights,
     out,
-    WA, WO, WU, WD, nrm, hid, p, q, mid32, mid, act,
+    WA, WO, WU, WD, nrm, hid, p, q, mid32, mid, act, fin,
     staged, leaving, gathered, detour,
-    rz, rd, re, sz, sd, sy, loc, rn, rb, rh, rt, sn, sh, st, r1, s1, ra, sa, r2, s2, ro, so,
+    rz, rd, re, sz, sd, sy, loc, rn, rb, rh, rt, sn, sh, st, r1, s1, ra, sa, r2, s2, ro, so, fo,
 ):
     packed, table, asc, taps, usc, oc, dc = gathered
     D = tok.shape[1]
@@ -566,10 +568,7 @@
     blocks = 2 * (nz - 1)
 
     def block(i):
-        rest = jnp.maximum(i - 2, 0)
-        near_in, late_in = jnp.where(i < 2, 1, 2 + rest % 2), jnp.where(i < 2, i, rest // 2)
-        near, late = jnp.where(inner, near_in, 1 + i // 2), jnp.where(inner, late_in, i % 2)
-        return place(near), (y + late) % 2
+        return place(1 + i // 2), (y + i) % 2
 
     def step(s, i):
         zs, yy = block(i)
@@ -647,7 +646,6 @@
 
     round_stage(0)
     round_stage(1)
-
     pl.semaphore_wait(barrier, G + T - 2 + jnp.where(outer, 2, 3))
     swap(0)
     send_in(0, f)
@@ -729,6 +727,10 @@
                 dc[zs, :, cols] = row_of[:, wide + ups + outs :]
     c = taps.shape[2]
 
+    def hand_over(gs):
+        here = pl.ds(off, rows)
+        copy(hid.at[G + gs, here], hid.at[gs, here], sh, rh.at[gs], (r, 2 * (z - inward) + y, t)).start()
+
     def project_far(lo, hi):
         @pl.loop(lo, hi)
         def _(k):
@@ -739,8 +741,7 @@
                 passed(G, rb)
 
             project(G, gs)
-            here = pl.ds(off, rows)
-            copy(hid.at[G + gs, here], hid.at[gs, here], sh, rh.at[gs], (r, 2 * (z - inward) + y, t)).start()
+            hand_over(gs)
 
     @pl.when(outer)
     def _():
@@ -775,7 +776,8 @@
         give_back(1)
         swapped(3)
         for ff in (f, fy):
-            spread(3, ff)
+            send(3, ff, across)
+            send_in(3, ff)
         both_to_siblings(3)
         steps(4, 0, blocks)
         steps(1, 0, blocks)
@@ -815,7 +817,7 @@
             project(0, gs)
     @pl.when(inner)
     def _():
-        project_far(0, 1)
+        project(G, g)
         pass_on(G, rb, True)
         pass_on(G, rb, False)
 
@@ -848,7 +850,7 @@
 
     @pl.loop(0, G)
     def _(k):
-        gs = nth(k)
+        gs = nth((k + 1) % G)
 
         @pl.when(outer)
         def _():
@@ -860,11 +862,11 @@
             h = hid[gs, pl.ds(off, rows), :]
             p[gs, ff] = jnp.dot(h, WO[ff], preferred_element_type=f32).astype(bf16)
 
-        @pl.when(outer & (k > 0) & (k < G - 1))
-        def _():
-            pl.loop(0, nz // 2)(lambda j: own_leg(j, k - 1))
-
-        @pl.when(outer & (k == G - 1))
+        @pl.when(outer & (k < 2))
+        def _():
+            pl.loop(0, nz // 2)(lambda j: own_leg(j, k))
+
+        @pl.when(outer & (k == 2))
         def _():
             pl.loop(0, nz)(pass_leg)
 
@@ -874,6 +876,7 @@
         for k in range(2):
             pl.loop(0, nz // 2)(lambda j: own_leg(j, k))
         project_far(3, G)
+        hand_over(g)
         inner_step(2, 1, 0)
         inner_step(2, 2, 0)
 
@@ -899,7 +902,6 @@
         both_to_siblings(2)
 
     pl.when(outer)(lambda: steps(2, 0, 1))
-
     @pl.loop(0, nz)
     def _(zs):
         for i in (0, 2):
@@ -923,7 +925,6 @@
 
     for m in (gx, gy):
         copy(mid.at[g], mid.at[g], sa, ra.at[g], member(m)).start()
-
     pl.when(outer)(lambda: steps(2, 2, 4))
 
     @pl.when(inner)
@@ -939,12 +940,12 @@
         arrived(mid.at[m], ra.at[m])
         some = mid.at[m, pl.ds(lo, part)]
         copy(some, some, sa, ra.at[m] if lo else ra.at[G], member(n)).start()
-
     pl.when(outer)(lambda: steps(2, 4, blocks))
 
     @pl.when(inner)
     def _():
         inner_step(3, 1, 0)
+        inner_step(3, 1, 1)
         inner_step(2, 3, 0)
         inner_step(2, 3, 1)
 
@@ -967,7 +968,9 @@
             upper = jnp.dot(x, WU[tt], preferred_element_type=f32) * usc[tt]
             act[gs, :, tt * u : (tt + 1) * u] = jnp.square(jnp.maximum(upper, 0.0)).astype(bf16)
 
-    pl.when(inner)(lambda: inner_step(3, 1, 1))
+    @pl.when(inner)
+    def _():
+        inner_step(3, 2, 0)
 
     def source(i):
         zs, yy = block(jnp.maximum(i - 2, 0))
@@ -975,8 +978,7 @@
         return zs, yy, 2 * zs + yy
 
     def direct(i):
-        zs, _, _ = source(i)
-        return outer & (zs == place(nz - 1))
+        return outer & (i > 3)
 
     def second_leg(i):
         _, _, ff = source(i)
@@ -1009,15 +1011,15 @@
                 acc = p[g, ff, at, :].astype(f32)
                 for m in slots:
                     acc = acc + q[m, ff, at, :].astype(f32)
-                here = pl.ds(pl.multiple_of(t * rows + k * TILE, TILE), TILE)
-                out[here, cols] = (mid32[zs, at, wide] + acc * dc[zs, :, wide]).astype(bf16)
+                fin[ff, at, :] = (mid32[zs, at, wide] + acc * dc[zs, :, wide]).astype(bf16)
 
         far = direct(i)
         pl.when(far)(lambda: sum_up((0, 1, 2)))
         pl.when(jnp.logical_not(far))(lambda: sum_up((0, 2)))
         mine = out.at[pl.ds(pl.multiple_of(t * rows, rows), rows), cols]
         for tt in siblings():
-            copy(mine, mine, so, ro, (r, f, tt)).start()
+            copy(fin.at[ff], mine, so, ro, (r, f, tt)).start()
+        pltpu.make_async_copy(fin.at[ff], mine, fo).start()
 
     @pl.loop(0, 2 * nz)
     def _(ff_at):
@@ -1027,8 +1029,8 @@
         def _():
             step(3, ff_at - 2)
 
-        for i, (near, late) in enumerate(((2, 0), (3, 0), (2, 1), (3, 1))):
-            pl.when(inner & (ff_at == 4 + i))(functools.partial(inner_step, 3, near, late))
+        for at, near, late in ((3, 2, 1), (6, 3, 0), (7, 3, 1)):
+            pl.when(inner & (ff_at == at))(functools.partial(inner_step, 3, near, late))
 
         from_siblings(3, ff)
 
@@ -1049,18 +1051,14 @@
         def _():
             second_leg(ff_at - 2)
 
-        @pl.when(ff_at > 3)
-        def _():
-            finish(ff_at - 4)
-
-    @pl.loop(2 * nz - 2, 2 * nz)
-    def _(i):
-        second_leg(i)
-        finish(i - 2)
-
-    @pl.loop(2 * nz - 2, 2 * nz)
-    def _(i):
-        finish(i)
+        @pl.when(ff_at > 5)
+        def _():
+            finish(ff_at - 6)
+
+    second_leg(2 * nz - 2)
+    pl.loop(2, 4)(finish)
+    second_leg(2 * nz - 1)
+    pl.loop(4, 2 * nz)(finish)
 
     for s in range(5):
         if s in (2, 3):
@@ -1102,7 +1100,9 @@
     half = out.at[pl.ds(0, rows)]
     for _ in siblings():
         arrived(half, ro)
-        arrived(half, so)
+        arrived(fin, so)
+    pltpu.make_async_copy(fin, fin, fo).wait()
+
 
 def body(
     R, n_fs, T,
@@ -1178,6 +1178,7 @@
             pltpu.VMEM((nz, rows, pw), f32),
             pltpu.VMEM((G, rows, D), bf16),
             pltpu.VMEM((G, rows, T * kd), bf16),
+            pltpu.VMEM((n_fs, rows, cw), bf16),
             *reading,
             tuple(pltpu.VMEM(shape, bf16) for shape in rounded[2:]),
             dma((5, n_fs)),
@@ -1199,6 +1200,7 @@
             dma((G + 1,)),
             dma,
             dma((G - 1, n_fs)),
+            dma,
             dma,
             dma,
             dma,
@@ -1237,11 +1239,12 @@
         functools.partial(run, nz, G, T, win, rows, inside),
         out_shape=jax.ShapeDtypeStruct((TOK, D), bf16),
         in_specs=[vmem] * 3 + [(vmem,) * len(vectors), (hbm,) * 6],
-        out_specs=vmem,
+        out_specs=hbm if lined else vmem,
         scratch_shapes=scratch,
         compiler_params=pltpu.CompilerParams(collective_id=0, has_side_effects=True, vmem_limit_bytes=limit),
     )(tokens[0], mix_gain[None], mlp_gain[None], vectors, weights)
     return result[None]
+
 
 def solution(mesh):
     placed = (

time: 177 us -> 170 us (0.960)
  Pallas kernels: 173 us -> 167 us
    pallas_call x1, Pallas kernels: 173 us -> 167 us  [body(): pl.pallas_call(functools.partial(run, nz, G, T, win, rows, inside), out_s...]
where the time goes in v4:
time: 170 us
  Pallas kernels  167 us (98%)
  local copies, waits for them, and re-layouts  2.73 us (2%)
    pallas_call x1, Pallas kernels, body(): pl.pallas_call(functools.partial(run, nz, G, T, win, rows, inside), out_s...  167 us

profile of v4, /device:TPU:0, one launch (start us, length us, event | category | flops | bytes accessed | tf_op | source)
XLA Modules:
  0.0 170.2 jit_solution(15334273308668607904)
XLA Ops:
  0.0 167.5 %shard_map.154 = bf16[384,2048]{1,0:T(8,128)(2,1)} custom-call(bf16[384,2048]{1,0:T(8,128)(2,1)} %bitcast.11, f32[1,2048]{1,0:T(1,128)} %bitcast.12, f32[1,2048]{1,0:T(1,128)} %bitcast.13, f32[1,128]{1,0:T(1,128)} %bitcast.17, f32[1,128]{1,0:T(1,128)} %bitcast.18, f32[1,128]{1,0:T(1,128)} %bitcast.19, f32[3,128]{1,0:T(4,128)} %bitcast.14, ...), custom_call_target="tpu_custom_call" | custom-call | tf_op jit(solution)/shard_map/pallas_call | solution.py:1238
  167.5 2.7 %copy.18 = bf16[1,384,2048]{2,1,0:T(8,128)(2,1)} copy(bf16[1,384,2048]{2,1,0:T(8,128)(2,1)} %bitcast.10) | data formatting | bytes 3145728

commit v5 on v4

--- a/solution.py
+++ b/solution.py
@@ -900,6 +900,7 @@
         swapped(2)
         send_in(2, fy)
         both_to_siblings(2)
+        inner_step(2, 2, 1)
 
     pl.when(outer)(lambda: steps(2, 0, 1))
     @pl.loop(0, nz)
@@ -923,31 +924,42 @@
             cols = slice(zs * pw, (zs + 1) * pw)
             mid[g, at, cols] = (mid32[zs, at, :] * inv * g2[:, cols]).astype(bf16)
 
-    for m in (gx, gy):
-        copy(mid.at[g], mid.at[g], sa, ra.at[g], member(m)).start()
-    pl.when(outer)(lambda: steps(2, 2, 4))
+    part = rows // 2
+
+    def half_of(m, h):
+        return mid.at[m, pl.ds(h * part, part)]
+
+    for h in range(2):
+        for m, way in ((gx, 1 - h), (gy, h)):
+            copy(half_of(g, way), half_of(g, way), sa, ra.at[g, way], member(m)).start()
+    @pl.when(outer)
+    def _():
+        steps(2, 2, 3)
+        steps(2, 4, 5)
+
 
     @pl.when(inner)
     def _():
-        inner_step(2, 2, 1)
+        inner_step(2, 1, 1)
+        inner_step(3, 1, 0)
         swapped(3)
         send_in(3, fy)
         both_to_siblings(3)
-        inner_step(2, 1, 1)
-
-    part = rows // 2
-    for m, n, lo in ((gx, gy, part), (gy, gx, 0)):
-        arrived(mid.at[m], ra.at[m])
-        some = mid.at[m, pl.ds(lo, part)]
-        copy(some, some, sa, ra.at[m] if lo else ra.at[G], member(n)).start()
-    pl.when(outer)(lambda: steps(2, 4, blocks))
+
+    for m, n, h in ((gx, gy, 1), (gy, gx, 0)):
+        arrived(half_of(m, h), ra.at[m, h])
+        copy(half_of(m, h), half_of(m, h), sa, ra.at[m, h], member(n)).start()
+    @pl.when(outer)
+    def _():
+        steps(2, 5, 6)
+        steps(2, 3, 4)
+
 
     @pl.when(inner)
     def _():
-        inner_step(3, 1, 0)
-        inner_step(3, 1, 1)
         inner_step(2, 3, 0)
         inner_step(2, 3, 1)
+        inner_step(3, 1, 1)
 
     all_from_siblings(2)
     u = usc.shape[2]
@@ -957,11 +969,13 @@
     def _(k):
         gs = nth(k)
 
-        @pl.when(k == G - 1)
-        def _():
-            some = mid.at[gd, pl.ds(0, part)]
-            arrived(some, ra.at[gd])
-            arrived(some, ra.at[G])
+        @pl.when((k == 1) | (k == G - 1))
+        def _():
+            arrived(half_of(gs, 0), ra.at[gs, 0])
+
+        @pl.when(k > 1)
+        def _():
+            arrived(half_of(gs, 1), ra.at[gs, 1])
 
         x = mid[gs]
         for tt in range(T):
@@ -978,7 +992,7 @@
         return zs, yy, 2 * zs + yy
 
     def direct(i):
-        return outer & (i > 3)
+        return outer & (i > 5)
 
     def second_leg(i):
         _, _, ff = source(i)
@@ -1025,6 +1039,10 @@
     def _(ff_at):
         _, _, ff = source(ff_at)
 
+        @pl.when(ff_at > 1)
+        def _():
+            second_leg(ff_at - 2)
+
         @pl.when(outer & (ff_at > 1) & (ff_at != 3))
         def _():
             step(3, ff_at - 2)
@@ -1034,22 +1052,26 @@
 
         from_siblings(3, ff)
 
-        @pl.loop(0, G)
-        def _(gs):
-            p[gs, ff] = jnp.dot(act[gs], WD[ff], preferred_element_type=f32).astype(bf16)
-
         first, second = legs(ff)
         far = direct(ff_at)
-        copy(p.at[gd, ff], q.at[1, ff], s2, r2.at[1, ff], member(jnp.where(far, gd, first))).start()
-        copy(p.at[first, ff], q.at[0, ff], s2, r2.at[0, ff], member(first)).start()
-
-        @pl.when(far)
-        def _():
-            copy(p.at[second, ff], q.at[2, ff], s2, r2.at[2, ff], member(second)).start()
-
-        @pl.when(ff_at > 1)
-        def _():
-            second_leg(ff_at - 2)
+
+        @pl.loop(0, G)
+        def _(k):
+            gs = jnp.where(k == 0, gd, jnp.where(k == 1, first, jnp.where(k == 2, second, g)))
+            p[gs, ff] = jnp.dot(act[gs], WD[ff], preferred_element_type=f32).astype(bf16)
+
+            @pl.when(k == 0)
+            def _():
+                to = member(jnp.where(far, gd, first))
+                copy(p.at[gd, ff], q.at[1, ff], s2, r2.at[1, ff], to).start()
+
+            @pl.when(k == 1)
+            def _():
+                copy(p.at[first, ff], q.at[0, ff], s2, r2.at[0, ff], member(first)).start()
+
+            @pl.when(far & (k == 2))
+            def _():
+                copy(p.at[second, ff], q.at[2, ff], s2, r2.at[2, ff], member(second)).start()
 
         @pl.when(ff_at > 5)
         def _():
@@ -1197,7 +1219,7 @@
             dma((2,)),
             dma((G - 1, nz)),
             dma,
-            dma((G + 1,)),
+            dma((G, 2)),
             dma,
             dma((G - 1, n_fs)),
             dma,

time: 170 us -> 170 us (level)
  no operation moved by 1% of the time
where the time goes in v5:
time: 170 us
  Pallas kernels  167 us (98%)
  local copies, waits for them, and re-layouts  2.73 us (2%)
    pallas_call x1, Pallas kernels, body(): pl.pallas_call(functools.partial(run, nz, G, T, win, rows, inside), out_s...  167 us

profile of v5, /device:TPU:0, one launch (start us, length us, event | category | flops | bytes accessed | tf_op | source)
XLA Modules:
  0.0 169.7 jit_solution(18340781562866813105)
XLA Ops:
  0.0 167.0 %shard_map.154 = bf16[384,2048]{1,0:T(8,128)(2,1)} custom-call(bf16[384,2048]{1,0:T(8,128)(2,1)} %bitcast.11, f32[1,2048]{1,0:T(1,128)} %bitcast.12, f32[1,2048]{1,0:T(1,128)} %bitcast.13, f32[1,128]{1,0:T(1,128)} %bitcast.17, f32[1,128]{1,0:T(1,128)} %bitcast.18, f32[1,128]{1,0:T(1,128)} %bitcast.19, f32[3,128]{1,0:T(4,128)} %bitcast.14, ...), custom_call_target="tpu_custom_call" | custom-call | tf_op jit(solution)/shard_map/pallas_call | solution.py:1260
  167.0 2.7 %copy.18 = bf16[1,384,2048]{2,1,0:T(8,128)(2,1)} copy(bf16[1,384,2048]{2,1,0:T(8,128)(2,1)} %bitcast.10) | data formatting | bytes 3145728

commit v6 on v5

--- a/solution.py
+++ b/solution.py
@@ -857,10 +857,11 @@
             some = hid.at[gs, pl.ds(off, rows)]
             arrived(some, rh.at[gs])
 
-        @pl.loop(0, 2 * nz)
-        def _(ff):
+        @pl.loop(0, nz // 2)
+        def _(j):
             h = hid[gs, pl.ds(off, rows), :]
-            p[gs, ff] = jnp.dot(h, WO[ff], preferred_element_type=f32).astype(bf16)
+            for i in range(4):
+                p[gs, 4 * j + i] = jnp.dot(h, WO[4 * j + i], preferred_element_type=f32).astype(bf16)
 
         @pl.when(outer & (k < 2))
         def _():

time: 170 us -> 169 us (level)
  no operation moved by 1% of the time
where the time goes in v6:
time: 169 us; the launch traced here: 168 us
  Pallas kernels  166 us (98%)
  local copies, waits for them, and re-layouts  2.73 us (2%)
    pallas_call x1, Pallas kernels, body(): pl.pallas_call(functools.partial(run, nz, G, T, win, rows, inside), out_s...  166 us

profile of v6, /device:TPU:0, one launch (start us, length us, event | category | flops | bytes accessed | tf_op | source)
XLA Modules:
  0.0 168.5 jit_solution(4838310102436378332)
XLA Ops:
  0.0 165.7 %shard_map.154 = bf16[384,2048]{1,0:T(8,128)(2,1)} custom-call(bf16[384,2048]{1,0:T(8,128)(2,1)} %bitcast.11, f32[1,2048]{1,0:T(1,128)} %bitcast.12, f32[1,2048]{1,0:T(1,128)} %bitcast.13, f32[1,128]{1,0:T(1,128)} %bitcast.17, f32[1,128]{1,0:T(1,128)} %bitcast.18, f32[1,128]{1,0:T(1,128)} %bitcast.19, f32[3,128]{1,0:T(4,128)} %bitcast.14, ...), custom_call_target="tpu_custom_call" | custom-call | tf_op jit(solution)/shard_map/pallas_call | solution.py:1261
  165.7 2.7 %copy.18 = bf16[1,384,2048]{2,1,0:T(8,128)(2,1)} copy(bf16[1,384,2048]{2,1,0:T(8,128)(2,1)} %bitcast.10) | data formatting | bytes 3145728
